TPU v7x, 32 devices: a whole 2x2x4 slice. The times are simulated.
32 devices in a mesh: sp: 8 (over z, x), tp: 4 (over y, core).
Axes of the slice: x: 2, y: 2, z: 4, core: 2. Of those that a mesh axis runs over, the one named last changes fastest.
Arguments:
- out_gate: bfloat16 [4096, 1536], P('sp', 'tp'), may hold values from -6 to 6
- in_gate: bfloat16 [4096, 1536], P('sp', 'tp'), may hold values from -6 to 6
- conv_values: bfloat16 [4096, 1536], P('sp', 'tp'), may hold values from -6 to 6
- conv_taps: float32 [3, 1536], P(None, 'tp'), may hold values from -3 to 3
- mix_gain: float32 [1536], replicated, may hold values from 0.1 to 1.9
- out_proj: bfloat16 [1536, 2048], replicated, may hold values from -0.15625 to 0.15625
- residual: bfloat16 [4096, 2048], P(('sp', 'tp')), may hold values from -6 to 6
- ffn_gain: float32 [2048], replicated, may hold values from 0.1 to 1.9
- routes: int32 [4096, 6], P(('sp', 'tp')), may hold values from 0 to 31, all different within a row; in each aligned block of 128 rows (0 to 127, 128 to 255, ...) at most 32 rows name the same one
- route_weights: float32 [4096, 6], P(('sp', 'tp')), may hold values from 0.05 to 1
- shared_gate: bfloat16 [2048, 512], replicated, may hold values from -0.125 to 0.125
- shared_up: bfloat16 [2048, 512], replicated, may hold values from -0.125 to 0.125
- shared_down: bfloat16 [512, 2048], replicated, may hold values from -0.25 to 0.25
- expert_gate: bfloat16 [32, 2048, 512], P(('sp', 'tp')), may hold values from -0.125 to 0.125
- expert_up: bfloat16 [32, 2048, 512], P(('sp', 'tp')), may hold values from -0.125 to 0.125
- expert_down: bfloat16 [32, 512, 2048], P(('sp', 'tp')), may hold values from -0.25 to 0.25
Outputs:
- layer_out: bfloat16 [4096, 2048], P(('sp', 'tp'))
Inputs may be any that keep to these rules, and one draw needn't show every extreme that they name: `routes`: each row names 6 different experts. Within the rows of one device (aligned blocks of 128 rows) no expert is named more than 32 times, a bound that some block reaches.
All inputs are finite; a program needn't handle non-finite values.
Results may differ from a plain program's by a relative error of at most 0.0065.
Values may be sent and summed in bfloat16 or wider, within the bound.
A program may use at most 128 MiB of HBM per device.

v0:
```python
import functools

import jax
import jax.numpy as jnp
from jax import lax
from jax.experimental import pallas as pl
from jax.experimental.pallas import tpu as pltpu
from jax.sharding import PartitionSpec as P

MESH = pl.DeviceIdType.MESH
META_ROWS = 16
HALO = 16


def ffn(x, gate, up, down):
    g = jnp.dot(x, gate[...], preferred_element_type=jnp.float32)
    u = jnp.dot(x, up[...], preferred_element_type=jnp.float32)
    h = (g / (1.0 + jnp.exp(-g)) * u).astype(jnp.bfloat16)
    return jnp.dot(h, down[...], preferred_element_type=jnp.float32)


def experts_kernel(
    n_sp, n_tp, width_x, cap, top,
    og_hbm, ig_hbm, cv_hbm, taps, mix_gain, residual, ffn_gain, routes, route_weights,
    op_hbm, eg_hbm, eu_hbm, ed_hbm, sg_hbm, su_hbm, sd_hbm,
    out,
    og, ig, cv, conv_out, conv_in, normed, meta_own,
    gathered, metas, staged, arrived, results, returned,
    left_in, right_in, total,
    op, eg, eu, ed, sg, su, sd,
    w_sem, halo_send, halo_recv, conv_send, conv_recv,
    meta_send, meta_recv, ring_send, ring_recv,
    disp_send, disp_recv, ret_send, ret_recv, red_send, red_recv,
):
    sp = lax.axis_index("sp")
    tp = lax.axis_index("tp")
    half = n_sp // 2
    rows, width = normed.shape
    length = og.shape[0]
    mid = rows // 2
    group = n_tp * cap
    width_z = n_sp // width_x

    def place_of(index):
        x, z = lax.rem(index, width_x), lax.div(index, width_x)
        return x * width_z + z + lax.rem(x, 2) * (width_z - 1 - 2 * z)

    def index_of(place):
        x, zz = lax.div(place, width_z), lax.rem(place, width_z)
        return (zz + lax.rem(x, 2) * (width_z - 1 - 2 * zz)) * width_x + x

    place = place_of(sp)

    def ahead(distance):
        return index_of(lax.rem(place + distance, n_sp))

    right, left = ahead(1), ahead(n_sp - 1)

    def partner(j):
        return lax.rem(tp + j, n_tp)

    barrier = pltpu.get_barrier_semaphore()
    for d in range(1, n_sp):
        pl.semaphore_signal(barrier, inc=1, device_id=(ahead(d), tp), device_id_type=MESH)
    for j in range(1, n_tp):
        pl.semaphore_signal(barrier, inc=1, device_id=(sp, partner(j)), device_id_type=MESH)

    weights = [
        pltpu.make_async_copy(src, dst, w_sem.at[i])
        for i, (src, dst) in enumerate(
            ((ig_hbm, ig.at[pl.ds(HALO, length)]), (cv_hbm, cv.at[pl.ds(HALO, length)]),
             (og_hbm, og), (op_hbm, op), (sg_hbm, sg), (su_hbm, su), (sd_hbm, sd),
             (eg_hbm.at[0], eg), (eu_hbm.at[0], eu), (ed_hbm.at[0], ed))
        )
    ]
    for copy in weights[:4]:
        copy.start()
    pl.semaphore_wait(barrier, n_sp - 1 + n_tp - 1)

    def remote(src, dst, send, recv, device):
        return pltpu.make_async_remote_copy(
            src_ref=src, dst_ref=dst, send_sem=send, recv_sem=recv,
            device_id=device, device_id_type=MESH,
        )

    def meta_copy(d):
        return remote(meta_own, metas.at[d], meta_send.at[d], meta_recv.at[d], (ahead(d), tp))

    def part_of(h):
        return pl.ds(h * mid, mid)

    def ring_copy(s, way, h, block=None):
        device = (right if way == 0 else left, tp)
        dst = gathered.at[s + 1 if way == 0 else n_sp - s - 1, part_of(h)]
        if block is None:
            src = gathered.at[s if way == 0 else lax.rem(n_sp - s, n_sp), part_of(h)]
        else:
            src = block.at[part_of(h)]
        return remote(src, dst, ring_send.at[way, s, h], ring_recv.at[way, s, h], device)

    def disp_copy(d, j):
        src = staged.at[d, pl.ds(pl.multiple_of(partner(j) * cap, cap), cap)]
        dst = arrived.at[d, pl.ds(pl.multiple_of(tp * cap, cap), cap)]
        return remote(src, dst, disp_send.at[d, j], disp_recv.at[d, j], (sp, partner(j)))

    def ret_copy(d, j):
        src = results.at[d, pl.ds(pl.multiple_of(partner(j) * cap, cap), cap)]
        dst = returned.at[d, pl.ds(pl.multiple_of(tp * cap, cap), cap)]
        return remote(src, dst, ret_send.at[d, j], ret_recv.at[d, j], (sp, partner(j)))

    def red_copy(s, way, h):
        device = (left if way == 0 else right, tp)
        src = gathered.at[s if way == 0 else n_sp - s, part_of(h)]
        dst = (left_in if way == 0 else right_in).at[s - 1, part_of(h)]
        return remote(src, dst, red_send.at[way, s, h], red_recv.at[way, s - 1, h], device)

    def halo_copy(i):
        src = (ig_hbm, cv_hbm)[i].at[pl.ds(length - HALO, HALO)]
        dst = (ig, cv)[i].at[pl.ds(0, HALO)]
        device = (lax.rem(sp + 1, n_sp), tp)
        return remote(src, dst, halo_send.at[i], halo_recv.at[i], device)

    def conv_copy(j):
        return remote(
            conv_out.at[j], conv_in.at[tp], conv_send.at[j], conv_recv.at[j], (sp, partner(j))
        )

    halo_copy(0).start()
    halo_copy(1).start()

    experts_total = n_sp * n_tp
    expert = lax.broadcasted_iota(jnp.int32, (experts_total, rows), 0)
    named = [routes[k : k + 1, :] == expert for k in range(top)]
    onehot = jnp.zeros((experts_total, rows), jnp.float32)
    for hit in named:
        onehot = jnp.where(hit, 1.0, onehot)
    earlier = lax.broadcasted_iota(jnp.int32, (rows, rows), 0) < lax.broadcasted_iota(
        jnp.int32, (rows, rows), 1
    )
    before = jnp.dot(
        onehot.astype(jnp.bfloat16),
        jnp.where(earlier, 1.0, 0.0).astype(jnp.bfloat16),
        preferred_element_type=jnp.float32,
    )
    slot = before + (expert * cap).astype(jnp.float32)
    meta_own[...] = jnp.zeros_like(meta_own)
    for k in range(top):
        meta_own[k : k + 1, :] = jnp.sum(jnp.where(named[k], slot, 0.0), axis=0, keepdims=True)
    weight = route_weights[...]
    meta_own[top : 2 * top, :] = weight / jnp.sum(weight, axis=0, keepdims=True) * 2.5

    for copy in weights[:3]:
        copy.wait()
    for copy in weights[4:7]:
        copy.start()
    for d in range(1, n_sp):
        meta_copy(d).start()
    halo_copy(0).wait_recv()
    halo_copy(1).wait_recv()
    taps_count = taps.shape[0]
    for j in list(range(1, n_tp)) + [0]:
        start = pl.multiple_of(partner(j) * rows, rows)
        span = pl.ds(start, rows + HALO)
        mixed = ig[span].astype(jnp.float32) * cv[span].astype(jnp.float32)
        blank = jnp.where(sp * n_tp + partner(j) == 0, HALO, 0)
        at = lax.broadcasted_iota(jnp.int32, mixed.shape, 0)
        mixed = jnp.where(at >= blank, mixed, 0.0)
        base = HALO - (taps_count - 1)
        filtered = taps[0:1, :] * mixed[base : base + rows]
        for o in range(1, taps_count):
            filtered = filtered + taps[o : o + 1, :] * mixed[base + o : base + o + rows]
        value = (og[pl.ds(start, rows)].astype(jnp.float32) * filtered).astype(jnp.bfloat16)
        if j == 0:
            conv_in[tp] = value
        else:
            conv_out[j] = value
            conv_copy(j).start()
    weights[3].wait()
    for copy in weights[7:]:
        copy.start()
    for j in range(1, n_tp):
        conv_copy(j).wait_recv()
    squares = jnp.zeros((rows, 1), jnp.float32)
    product = jnp.zeros((rows, width), jnp.float32)
    part_width = conv_in.shape[2]
    for t in range(n_tp):
        value = conv_in[t].astype(jnp.float32)
        squares = squares + jnp.sum(value * value, axis=1, keepdims=True)
        product = product + jnp.dot(
            (value * mix_gain[t]).astype(jnp.bfloat16),
            op[t * part_width : (t + 1) * part_width, :],
            preferred_element_type=jnp.float32,
        )
    inverse = lax.rsqrt(squares / (n_tp * part_width) + 1e-06)
    stream = residual[...].astype(jnp.float32) + product * inverse
    power = jnp.mean(stream * stream, axis=1, keepdims=True)
    normed[...] = (stream * lax.rsqrt(power + 1e-06) * ffn_gain[...]).astype(jnp.bfloat16)
    total[...] = stream

    first_slot = (sp * group).astype(jnp.float32)

    def matches(meta, k):
        slots = lax.broadcasted_iota(jnp.int32, (group, rows), 0).astype(jnp.float32) + first_slot
        return slots == meta[k : k + 1, :]

    def dispatch(d, block, meta):
        pick = jnp.zeros((group, rows), jnp.float32)
        for k in range(top):
            pick = jnp.where(matches(meta, k), 1.0, pick)
        staged[d] = jnp.dot(
            pick.astype(jnp.bfloat16), block, preferred_element_type=jnp.float32
        ).astype(jnp.bfloat16)
        for j in range(1, n_tp):
            disp_copy(d, j).start()

    own = pl.ds(pl.multiple_of(tp * cap, cap), cap)

    def run_expert(d):
        for j in range(1, n_tp):
            disp_copy(d, j).wait_recv()
        arrived[d, own] = staged[d, own]
        results[d] = ffn(arrived[d], eg, eu, ed).astype(jnp.bfloat16)

    def combine(d, meta):
        for j in range(1, n_tp):
            ret_copy(d, j).wait_recv()
        returned[d, own] = results[d, own]
        mix = jnp.zeros((group, rows), jnp.float32)
        for k in range(top):
            mix = jnp.where(matches(meta, k), meta[top + k : top + k + 1, :], mix)
        return lax.dot_general(
            mix.astype(jnp.bfloat16), returned[d], (((0,), (0,)), ((), ())),
            preferred_element_type=jnp.float32,
        )

    for h in range(2):
        for way in range(2):
            ring_copy(0, way, way if h == 0 else 1 - way, normed).start()
    dispatch(0, normed[...], meta_own[...])
    left_in[half - 1, mid:] = jnp.zeros((rows - mid, normed.shape[1]), jnp.bfloat16)
    right_in[half - 1, :mid] = jnp.zeros((mid, normed.shape[1]), jnp.bfloat16)
    for copy in weights[4:7]:
        copy.wait()
    total[...] += ffn(normed[...], sg, su, sd)
    for copy in weights[7:]:
        copy.wait()

    def gather_step(s, carry):
        for order in range(2):
            for way in range(2):
                h = way if order == 0 else 1 - way
                ring_copy(s - 1, way, h).wait_recv()
                if order == 0:
                    ring_copy(s, way, h).start()
                else:

                    @pl.when(s < half - 1)
                    def _():
                        ring_copy(s, way, h).start()

        def one(i, c):
            d = s + i * (n_sp - 2 * s)
            meta_copy(d).wait_recv()
            dispatch(d, gathered[d], metas[d])
            return c

        lax.fori_loop(0, 2, one, 0)

        @pl.when(s == 1)
        def _():
            run_expert(0)

        @pl.when(s > 1)
        def _():
            def two(i, c):
                run_expert(s - 1 + i * (n_sp - 2 * (s - 1)))
                return c

            lax.fori_loop(0, 2, two, 0)

        return carry

    lax.fori_loop(1, half, gather_step, 0)
    ring_copy(half - 1, 0, 0).wait_recv()
    ring_copy(half - 1, 1, 1).wait_recv()
    meta_copy(half).wait_recv()
    dispatch(half, gathered[half], metas[half])

    def give_back(d):
        for j in range(1, n_tp):
            ret_copy(d, j).start()

    def last(i, c):
        d = half - 1 + 2 * i - 3 * lax.div(i, 2)
        run_expert(d)
        give_back(d)
        return c

    lax.fori_loop(0, 3, last, 0)
    for s in range(half - 2, 0, -1):
        give_back(s)
        give_back(n_sp - s)
    give_back(0)

    for way in range(2):
        for h in range(2):
            ring_copy(0, way, h, normed).wait_send()
            for s in range(1, half - 1):
                ring_copy(s, way, h).wait_send()
        ring_copy(half - 1, way, way).wait_send()
    part = combine(half, metas[half])
    gathered[half] = part.astype(jnp.bfloat16)
    red_copy(half, 0, 0).start()
    red_copy(half, 1, 1).start()

    def reduce_step(i, carry):
        s = half - 1 - i
        for way, (d, buf_in) in enumerate(((s, left_in), (n_sp - s, right_in))):
            part = combine(d, metas[d])

            for order in range(2):
                h = way if order == 0 else 1 - way
                if order == 0:
                    red_copy(s + 1, way, h).wait_recv()
                else:

                    @pl.when(s < half - 1)
                    def _():
                        red_copy(s + 1, way, h).wait_recv()

                at = slice(h * mid, (h + 1) * mid)
                gathered[d, at] = (part[at] + buf_in[s, at].astype(jnp.float32)).astype(
                    jnp.bfloat16
                )
                red_copy(s, way, h).start()
        return carry

    lax.fori_loop(0, half - 1, reduce_step, 0)
    part = combine(0, meta_own[...]) + total[...]
    for way, buf_in in enumerate((left_in, right_in)):
        for h in range(2):
            red_copy(1, way, h).wait_recv()
        part = part + buf_in[0].astype(jnp.float32)
    out[...] = part.astype(out.dtype)

    for d in range(1, n_sp):
        meta_copy(d).wait_send()
    for j in range(1, n_tp):
        conv_copy(j).wait_send()
    for way in range(2):
        halo_copy(way).wait_send()
        red_copy(half, way, way).wait_send()
        for s in range(1, half):
            for h in range(2):
                red_copy(s, way, h).wait_send()

    def drain(d, c):
        for j in range(1, n_tp):
            disp_copy(d, j).wait_send()
            ret_copy(d, j).wait_send()
        return c

    lax.fori_loop(0, n_sp, drain, 0)


def body(
    out_gate,
    in_gate,
    conv_values,
    conv_taps,
    mix_gain,
    out_proj,
    residual,
    ffn_gain,
    routes,
    route_weights,
    shared_gate,
    shared_up,
    shared_down,
    expert_gate,
    expert_up,
    expert_down,
):
    n_sp, n_tp = lax.axis_size("sp"), lax.axis_size("tp")
    length, channels = in_gate.shape
    rows, width = residual.shape
    top = routes.shape[1]
    cap = max(2, 4 * rows * top // (3 * n_sp * n_tp))
    hidden, shared_hidden = expert_gate.shape[-1], shared_gate.shape[-1]
    half = n_sp // 2
    group = n_tp * cap
    width_x = max(1, n_tp // 2)
    if n_sp % width_x:
        width_x = 1
    bf, f32 = jnp.bfloat16, jnp.float32
    vmem = pl.BlockSpec(memory_space=pltpu.VMEM)
    anywhere = pl.BlockSpec(memory_space=pl.ANY)
    dma = pltpu.SemaphoreType.DMA
    return pl.pallas_call(
        functools.partial(experts_kernel, n_sp, n_tp, width_x, cap, top),
        out_shape=jax.ShapeDtypeStruct((rows, width), bf),
        in_specs=[anywhere] * 3 + [vmem] * 6 + [anywhere] * 7,
        out_specs=vmem,
        scratch_shapes=[
            pltpu.VMEM((length, channels), bf),
            pltpu.VMEM((length + HALO, channels), bf),
            pltpu.VMEM((length + HALO, channels), bf),
            pltpu.VMEM((n_tp, rows, channels), bf),
            pltpu.VMEM((n_tp, rows, channels), bf),
            pltpu.VMEM((rows, width), bf),
            pltpu.VMEM((META_ROWS, rows), f32),
            pltpu.VMEM((n_sp, rows, width), bf),
            pltpu.VMEM((n_sp, META_ROWS, rows), f32),
            pltpu.VMEM((n_sp, group, width), bf),
            pltpu.VMEM((n_sp, group, width), bf),
            pltpu.VMEM((n_sp, group, width), bf),
            pltpu.VMEM((n_sp, group, width), bf),
            pltpu.VMEM((half, rows, width), bf),
            pltpu.VMEM((half, rows, width), bf),
            pltpu.VMEM((rows, width), f32),
            pltpu.VMEM((n_tp * channels, width), bf),
            pltpu.VMEM((width, hidden), bf),
            pltpu.VMEM((width, hidden), bf),
            pltpu.VMEM((hidden, width), bf),
            pltpu.VMEM((width, shared_hidden), bf),
            pltpu.VMEM((width, shared_hidden), bf),
            pltpu.VMEM((shared_hidden, width), bf),
            dma((10,)),
            dma((2,)),
            dma((2,)),
            dma((n_tp,)),
            dma((n_tp,)),
            dma((n_sp,)),
            dma((n_sp,)),
            dma((2, half, 2)),
            dma((2, half, 2)),
            dma((n_sp, n_tp)),
            dma((n_sp, n_tp)),
            dma((n_sp, n_tp)),
            dma((n_sp, n_tp)),
            dma((2, half + 1, 2)),
            dma((2, half + 1, 2)),
        ],
        compiler_params=pltpu.CompilerParams(
            collective_id=0, has_side_effects=True, vmem_limit_bytes=63 * 1024 * 1024
        ),
    )(
        out_gate, in_gate, conv_values, conv_taps, mix_gain.reshape(n_tp, 1, channels),
        residual, ffn_gain.reshape(1, width), routes.T, route_weights.T,
        out_proj, expert_gate, expert_up, expert_down, shared_gate, shared_up, shared_down,
    )


def solution(mesh):
    in_specs = (
        P("sp", "tp"),
        P("sp", "tp"),
        P("sp", "tp"),
        P(None, "tp"),
        P(),
        P(),
        P(("sp", "tp"), None),
        P(),
        P(("sp", "tp"), None),
        P(("sp", "tp"), None),
        P(),
        P(),
        P(),
        P(("sp", "tp"), None, None),
        P(("sp", "tp"), None, None),
        P(("sp", "tp"), None, None),
    )
    out_specs = P(("sp", "tp"), None)
    return jax.shard_map(body, mesh=mesh, in_specs=in_specs, out_specs=out_specs, check_vma=False)
```

profile of v0, /device:TPU:0, one launch (start us, length us, event | category | flops | bytes accessed | tf_op | source)
XLA Modules:
  0.0 134.5 jit_solution(12061789201748988268)
XLA Ops:
  0.0 1.3 reshape.6.mix_gain
  1.3 131.3 %shard_map.154 = bf16[128,2048]{1,0:T(8,128)(2,1)} custom-call(bf16[512,384]{1,0:T(8,128)(2,1)} %og_hbm.1, bf16[512,384]{1,0:T(8,128)(2,1)} %ig_hbm.1, bf16[512,384]{1,0:T(8,128)(2,1)} %cv_hbm.1, f32[3,384]{1,0:T(4,128)} %taps.1, f32[4,1,384]{2,1,0:T(1,128)} %reshape.6.mix_gain, bf16[128,2048]{1,0:T(8,128)(2,1)} %residual.1, f32[1,2048]{1,0:T(1,128)} %bitcast.3, ...), custom_call_target="tpu_custom_call" | custom-call | tf_op jit(solution)/shard_map/pallas_call | solution.py:399
  132.6 1.9 %copy.18 = bf16[128,2048]{1,0:T(8,128)(2,1)} copy(bf16[128,2048]{1,0:T(8,128)(2,1)} %shard_map.154) | data formatting | bytes 1048576
where the time goes:
time: 135 us
  Pallas kernels  131 us (97%)
  local copies, waits for them, and re-layouts  3.18 us (2%)
    pallas_call x1, Pallas kernels, body(): pl.pallas_call(functools.partial(experts_kernel, n_sp, n_tp, width_x, cap...  131 us

commit v1 on v0

v1 whole, which is shorter than its diff:
```python
import functools

import jax
import jax.numpy as jnp
from jax import lax
from jax.experimental import pallas as pl
from jax.experimental.pallas import tpu as pltpu
from jax.sharding import PartitionSpec as P

MESH = pl.DeviceIdType.MESH
META_ROWS = 16
HALO = 16


def ffn(x, gate, up, down):
    g = jnp.dot(x, gate[...], preferred_element_type=jnp.float32)
    u = jnp.dot(x, up[...], preferred_element_type=jnp.float32)
    h = (g / (1.0 + jnp.exp(-g)) * u).astype(jnp.bfloat16)
    return jnp.dot(h, down[...], preferred_element_type=jnp.float32)


def experts_kernel(
    n_sp, n_tp, lag, cap, top,
    og_hbm, ig_hbm, cv_hbm, taps, mix_gain, residual, ffn_gain, routes, route_weights,
    op_hbm, eg_hbm, eu_hbm, ed_hbm, sg_hbm, su_hbm, sd_hbm,
    out,
    og, ig, cv, conv_out, conv_in,
    gathered, metas, staged, arrived, results, returned,
    left_in, right_in, total,
    op, eg, eu, ed, sg, su, sd,
    w_sem, halo_send, halo_recv, conv_send, conv_recv,
    meta_send, meta_recv, ring_send, ring_recv,
    disp_send, disp_recv, ret_send, ret_recv, red_send, red_recv,
):
    sp = lax.axis_index("sp")
    tp = lax.axis_index("tp")
    half = n_sp // 2
    rows, width = total.shape
    length = og.shape[0]
    mid = rows // 2
    group = n_tp * cap
    wide = n_tp // 2
    batch = wide * cap
    depth = n_sp // wide
    x, z = lax.rem(sp, wide), lax.div(sp, wide)
    y, core = lax.div(tp, 2), lax.rem(tp, 2)

    def across(kind):
        return y + kind * (x - y)

    def along(kind):
        return x + kind * (y - x)

    def device_at(kind, ring_index, member_index):
        zz, aa = lax.div(ring_index, wide), lax.rem(ring_index, wide)
        bb, cc = lax.div(member_index, 2), lax.rem(member_index, 2)
        return zz * wide + aa + kind * (bb - aa), (bb + kind * (aa - bb)) * 2 + cc

    ring = z * wide + along(core)
    member = across(core) * 2 + core

    def place_of(index):
        a, zz = lax.rem(index, wide), lax.div(index, wide)
        return a * depth + zz + lax.rem(a, 2) * (depth - 1 - 2 * zz)

    def index_of(place):
        a, zz = lax.div(place, depth), lax.rem(place, depth)
        return (zz + lax.rem(a, 2) * (depth - 1 - 2 * zz)) * wide + a

    place = place_of(ring)

    def ahead(distance):
        return device_at(core, index_of(lax.rem(place + distance, n_sp)), member)

    right, left = ahead(1), ahead(n_sp - 1)

    barrier = pltpu.get_barrier_semaphore()

    def greet(device):
        pl.semaphore_signal(barrier, inc=1, device_id=device, device_id_type=MESH)

    for d in range(1, n_sp):
        greet(ahead(d))
    for j in range(1, n_tp):
        greet((sp, lax.rem(tp + j, n_tp)))
        greet(device_at(1, z * wide + y, lax.rem(x * 2 + core + j, n_tp)))
    greet((lax.rem(sp + 1, n_sp), tp))
    greet((lax.rem(sp + n_sp - 1, n_sp), tp))

    weights = [
        pltpu.make_async_copy(src, dst, w_sem.at[i])
        for i, (src, dst) in enumerate(
            ((ig_hbm, ig.at[pl.ds(HALO, length)]), (cv_hbm, cv.at[pl.ds(HALO, length)]),
             (og_hbm, og), (op_hbm, op), (sg_hbm, sg), (su_hbm, su), (sd_hbm, sd),
             (eg_hbm.at[0], eg), (eu_hbm.at[0], eu), (ed_hbm.at[0], ed))
        )
    ]
    for copy in weights[:4]:
        copy.start()

    def remote(src, dst, send, recv, device):
        return pltpu.make_async_remote_copy(
            src_ref=src, dst_ref=dst, send_sem=send, recv_sem=recv,
            device_id=device, device_id_type=MESH,
        )

    def meta_copy(d):
        return remote(metas.at[0], metas.at[d], meta_send.at[d], meta_recv.at[d], ahead(d))

    def part_of(h):
        return pl.ds(h * mid, mid)

    def ring_copy(s, way, h):
        dst = gathered.at[s + 1 if way == 0 else n_sp - s - 1, part_of(h)]
        src = gathered.at[s if way == 0 else lax.rem(n_sp - s, n_sp), part_of(h)]
        device = right if way == 0 else left
        return remote(src, dst, ring_send.at[way, s, h], ring_recv.at[way, s, h], device)

    def slots(index):
        return pl.ds(pl.multiple_of(index * cap, cap), cap)

    def disp_copy(p, j):
        to = lax.rem(member + j, n_tp)
        return remote(
            staged.at[p, slots(to)], arrived.at[core, slots(p * wide + across(core))],
            disp_send.at[p, j], disp_recv.at[core, p, across(core)], device_at(core, ring, to),
        )

    def is_own(kind, b):
        return jnp.logical_and(core == kind, across(kind) == b)

    def holder(kind, b):
        return device_at(kind, z * wide + along(kind), b * 2 + kind)

    def disp_arrival(kind, p, b):
        return remote(
            staged.at[p, slots(0)], arrived.at[kind, slots(p * wide + b)],
            disp_send.at[p, 0], disp_recv.at[kind, p, b], holder(kind, b),
        )

    def ret_copy(kind, p, b):
        me = across(kind) * 2 + core
        return remote(
            results.at[kind, slots(p * wide + b)], returned.at[p, slots(me)],
            ret_send.at[kind, p, b], ret_recv.at[p, me], holder(kind, b),
        )

    def ret_arrival(p, j):
        frm = lax.rem(member + j, n_tp)
        return remote(
            results.at[0, slots(0)], returned.at[p, slots(frm)],
            ret_send.at[0, p, 0], ret_recv.at[p, frm], device_at(core, ring, frm),
        )

    def red_copy(s, way, h):
        device = left if way == 0 else right
        src = gathered.at[s if way == 0 else n_sp - s, part_of(h)]
        dst = (left_in if way == 0 else right_in).at[s - 1, part_of(h)]
        return remote(src, dst, red_send.at[way, s, h], red_recv.at[way, s - 1, h], device)

    def halo_copy(i):
        buf = (ig, cv)[i]
        device = (lax.rem(sp + 1, n_sp), tp)
        return remote(
            buf.at[pl.ds(length, HALO)], buf.at[pl.ds(0, HALO)],
            halo_send.at[i], halo_recv.at[i], device,
        )

    def conv_copy(t):
        return remote(
            conv_out.at[t], conv_in.at[tp], conv_send.at[t], conv_recv.at[tp], (sp, t)
        )

    def conv_arrival(t):
        return remote(conv_out.at[t], conv_in.at[t], conv_send.at[t], conv_recv.at[t], (sp, t))

    experts_total = n_sp * n_tp
    expert = lax.broadcasted_iota(jnp.int32, (experts_total, rows), 0)
    named = [routes[k : k + 1, :] == expert for k in range(top)]
    onehot = jnp.zeros((experts_total, rows), jnp.float32)
    for hit in named:
        onehot = jnp.where(hit, 1.0, onehot)
    earlier = lax.broadcasted_iota(jnp.int32, (rows, rows), 0) < lax.broadcasted_iota(
        jnp.int32, (rows, rows), 1
    )
    before = jnp.dot(
        onehot.astype(jnp.bfloat16),
        jnp.where(earlier, 1.0, 0.0).astype(jnp.bfloat16),
        preferred_element_type=jnp.float32,
    )

    def split(value, by):
        high = jnp.floor((value + 0.5) / by)
        return high, value - high * by

    rest, ec = split(expert.astype(jnp.float32), 2)
    rest, ey = split(rest, wide)
    ez, ex = split(rest, wide)
    turn = core.astype(jnp.float32)
    ea, eb = ex + turn * (ey - ex), ey + turn * (ex - ey)
    slot = before + ((ez * wide + ea) * n_tp + eb * 2 + ec) * cap
    metas[0] = jnp.zeros(metas.shape[1:], jnp.float32)
    for k in range(top):
        metas[0, k : k + 1, :] = jnp.sum(jnp.where(named[k], slot, 0.0), axis=0, keepdims=True)
    weight = route_weights[...]
    metas[0, top : 2 * top, :] = weight / jnp.sum(weight, axis=0, keepdims=True) * 2.5

    for copy in weights[:3]:
        copy.wait()
    with jax.named_scope("barrier"):
        pl.semaphore_wait(barrier, n_sp - 1 + 2 * (n_tp - 1) + 2)
    halo_copy(0).start()
    halo_copy(1).start()
    for copy in weights[4:7]:
        copy.start()

    taps_count = taps.shape[0]
    owners = [t for t in range(2, n_tp, 2)] + [t for t in range(1, n_tp, 2)] + [0]
    for t in owners:
        if t == 0:
            with jax.named_scope("halo_wait"):
                halo_copy(0).wait_recv()
                halo_copy(1).wait_recv()
        span = pl.ds(t * rows, rows + HALO)
        mixed = ig[span].astype(jnp.float32) * cv[span].astype(jnp.float32)
        if t == 0:
            blank = jnp.where(sp == 0, HALO, 0)
            at = lax.broadcasted_iota(jnp.int32, mixed.shape, 0)
            mixed = jnp.where(at >= blank, mixed, 0.0)
        base = HALO - (taps_count - 1)
        filtered = taps[0:1, :] * mixed[base : base + rows]
        for o in range(1, taps_count):
            filtered = filtered + taps[o : o + 1, :] * mixed[base + o : base + o + rows]
        value = (og[pl.ds(t * rows, rows)].astype(jnp.float32) * filtered).astype(jnp.bfloat16)
        conv_out[t] = value

        @pl.when(tp != t)
        def _():
            conv_copy(t).start()

    for d in range(1, n_sp):
        meta_copy(d).start()
    weights[3].wait()
    for copy in weights[7:]:
        copy.start()

    squares = jnp.zeros((rows, 1), jnp.float32)
    product = jnp.zeros((rows, width), jnp.float32)
    part_width = conv_in.shape[2]
    sources = [tp, tp + 1 - 2 * core]
    for i in range(1, wide):
        other = lax.rem(y + i, wide) * 2
        sources += [other, other + 1]
    for i, t in enumerate(sources):
        if i == 0:
            value = conv_out[t].astype(jnp.float32)
        else:
            with jax.named_scope("conv_wait"):
                conv_arrival(t).wait_recv()
            value = conv_in[t].astype(jnp.float32)
        gain = mix_gain[:, :part_width]
        for k in range(1, n_tp):
            gain = jnp.where(t == k, mix_gain[:, k * part_width : (k + 1) * part_width], gain)
        squares = squares + jnp.sum(value * value, axis=1, keepdims=True)
        product = product + jnp.dot(
            (value * gain).astype(jnp.bfloat16),
            op[pl.ds(pl.multiple_of(t * part_width, part_width), part_width), :],
            preferred_element_type=jnp.float32,
        )
    inverse = lax.rsqrt(squares / (n_tp * part_width) + 1e-06)
    stream = residual[...].astype(jnp.float32) + product * inverse
    power = jnp.mean(stream * stream, axis=1, keepdims=True)
    gathered[0] = (stream * lax.rsqrt(power + 1e-06) * ffn_gain[...]).astype(jnp.bfloat16)
    total[...] = stream

    first_slot = (ring * group).astype(jnp.float32)

    def matches(meta, k):
        at = lax.broadcasted_iota(jnp.int32, (group, rows), 0).astype(jnp.float32) + first_slot
        return at == meta[k : k + 1, :]

    def dispatch(d, p):
        meta = metas[d]
        pick = jnp.zeros((group, rows), jnp.float32)
        for k in range(top):
            pick = jnp.where(matches(meta, k), 1.0, pick)
        staged[p] = jnp.dot(
            pick.astype(jnp.bfloat16), gathered[d], preferred_element_type=jnp.float32
        ).astype(jnp.bfloat16)
        for j in range(1, n_tp):
            disp_copy(p, j).start()
        arrived[core, slots(p * wide + across(core))] = staged[p, slots(member)]

    def gather_action(a):
        @pl.when(a == 0)
        def _():
            for h in range(2):
                for way in range(2):
                    ring_copy(0, way, way if h == 0 else 1 - way).start()

        @pl.when(a > 0)
        def _():
            for way in range(2):
                with jax.named_scope("ring_wait"):
                    ring_copy(a - 1, way, way).wait_recv()

                @pl.when(a < half)
                def _():
                    ring_copy(a, way, way).start()

            @pl.when(a < half)
            def _():
                for way in range(2):
                    with jax.named_scope("ring_wait"):
                        ring_copy(a - 1, way, 1 - way).wait_recv()

                    @pl.when(a < half - 1)
                    def _():
                        ring_copy(a, way, 1 - way).start()

        def one(i, c):
            d = a + i * (n_sp - 2 * a)

            @pl.when(d > 0)
            def _():
                meta_copy(d).wait_recv()

            with jax.named_scope("dispatch"):
                dispatch(d, jnp.maximum(2 * a - 1, 0) + i)
            return c

        count = jnp.where(jnp.logical_or(a == 0, a == half), 1, 2)
        lax.fori_loop(0, count, one, 0)

    def run_expert(kind, p, count):
        with jax.named_scope("disp_wait"):
            for i in range(count):
                for b in range(wide):
                    @pl.when(jnp.logical_not(is_own(kind, b)))
                    def _():
                        disp_arrival(kind, p + i, b).wait_recv()

        span = pl.ds(pl.multiple_of(p * batch, batch), count * batch)
        with jax.named_scope("ffn"):
            results[kind, span] = ffn(arrived[kind, span], eg, eu, ed).astype(jnp.bfloat16)

    def give_back(kind, p):
        for b in range(wide):
            own = is_own(kind, b)

            @pl.when(jnp.logical_not(own))
            def _():
                ret_copy(kind, p, b).start()

            @pl.when(own)
            def _():
                returned[p, slots(member)] = results[kind, slots(p * wide + b)]

    def expert_action(kind, u):
        @pl.when(jnp.logical_and(u > 1, u <= half))
        def _():
            run_expert(kind, 2 * u - 3, 2)

        @pl.when(jnp.logical_or(u == 1, u == half))
        def _():
            run_expert(kind, jnp.where(u == 1, 0, n_sp - 1), 1)

        @pl.when(u == half)
        def _():
            give_back(kind, n_sp - 1)

        @pl.when(jnp.logical_and(u >= half, u <= 2 * half - 2))
        def _():
            give_back(kind, 4 * half - 3 - 2 * u)
            give_back(kind, 4 * half - 2 - 2 * u)

        @pl.when(u == 2 * half - 2)
        def _():
            give_back(kind, 0)

    def combine(d, p):
        with jax.named_scope("ret_wait"):
            for j in range(1, n_tp):
                ret_arrival(p, j).wait_recv()
        meta = metas[d]
        mix = jnp.zeros((group, rows), jnp.float32)
        for k in range(top):
            mix = jnp.where(matches(meta, k), meta[top + k : top + k + 1, :], mix)
        return lax.dot_general(
            mix.astype(jnp.bfloat16), returned[p], (((0,), (0,)), ((), ())),
            preferred_element_type=jnp.float32,
        )

    def reduce_start():
        for way in range(2):
            for h in range(2):
                for s in range(half - 1 if h != way else half):
                    ring_copy(s, way, h).wait_send()
        gathered[half] = combine(half, n_sp - 1).astype(jnp.bfloat16)
        red_copy(half, 0, 0).start()
        red_copy(half, 1, 1).start()

    def reduce_step(s):
        for way, buf_in in enumerate((left_in, right_in)):
            d, p = (s, 2 * s - 1) if way == 0 else (n_sp - s, 2 * s)
            part = combine(d, p)
            for order in range(2):
                h = way if order == 0 else 1 - way
                if order == 0:
                    with jax.named_scope("red_wait"):
                        red_copy(s + 1, way, h).wait_recv()
                else:

                    @pl.when(s < half - 1)
                    def _():
                        with jax.named_scope("red_wait2"):
                            red_copy(s + 1, way, h).wait_recv()

                at = slice(h * mid, (h + 1) * mid)
                gathered[d, at] = (part[at] + buf_in[s, at].astype(jnp.float32)).astype(
                    jnp.bfloat16
                )
                red_copy(s, way, h).start()

    def finish():
        part = combine(0, 0) + total[...]
        for way, buf_in in enumerate((left_in, right_in)):
            with jax.named_scope("red_wait_last"):
                for h in range(2):
                    red_copy(1, way, h).wait_recv()
            part = part + buf_in[0].astype(jnp.float32)
        out[...] = part.astype(out.dtype)

    left_in[half - 1, mid:] = jnp.zeros((rows - mid, width), jnp.bfloat16)
    right_in[half - 1, :mid] = jnp.zeros((mid, width), jnp.bfloat16)

    def step(k, carry):
        a = k - lag * core

        @pl.when(jnp.logical_and(a >= 0, a <= half))
        def _():
            gather_action(a)

        @pl.when(k == 0)
        def _():
            for copy in weights[4:7]:
                copy.wait()
            with jax.named_scope("shared"):
                total[...] += ffn(gathered[0], sg, su, sd)
            for copy in weights[7:]:
                copy.wait()

        def kinds(kind, c):
            expert_action(kind, k - lag * kind)
            return c

        lax.fori_loop(0, 2, kinds, 0)

        @pl.when(a == half + 1)
        def _():
            reduce_start()

        @pl.when(jnp.logical_and(a > half + 1, a <= 2 * half))
        def _():
            reduce_step(2 * half + 1 - a)

        @pl.when(a == 2 * half + 1)
        def _():
            finish()

        return carry

    lax.fori_loop(0, lag + 2 * half + 2, step, 0)

    for d in range(1, n_sp):
        meta_copy(d).wait_send()
    for t in range(n_tp):

        @pl.when(tp != t)
        def _():
            conv_copy(t).wait_send()

    for way in range(2):
        halo_copy(way).wait_send()
        red_copy(half, way, way).wait_send()
        for s in range(1, half):
            for h in range(2):
                red_copy(s, way, h).wait_send()

    def drain(p, c):
        for j in range(1, n_tp):
            disp_copy(p, j).wait_send()
        for kind in range(2):
            for b in range(wide):

                @pl.when(jnp.logical_not(is_own(kind, b)))
                def _():
                    ret_copy(kind, p, b).wait_send()

        return c

    lax.fori_loop(0, n_sp, drain, 0)


def body(
    out_gate,
    in_gate,
    conv_values,
    conv_taps,
    mix_gain,
    out_proj,
    residual,
    ffn_gain,
    routes,
    route_weights,
    shared_gate,
    shared_up,
    shared_down,
    expert_gate,
    expert_up,
    expert_down,
):
    n_sp, n_tp = lax.axis_size("sp"), lax.axis_size("tp")
    length, channels = in_gate.shape
    rows, width = residual.shape
    top = routes.shape[1]
    cap = max(2, 4 * rows * top // (3 * n_sp * n_tp))
    hidden, shared_hidden = expert_gate.shape[-1], shared_gate.shape[-1]
    half = n_sp // 2
    group = n_tp * cap
    wide = n_tp // 2
    lag = 0
    bf, f32 = jnp.bfloat16, jnp.float32
    vmem = pl.BlockSpec(memory_space=pltpu.VMEM)
    anywhere = pl.BlockSpec(memory_space=pl.ANY)
    dma = pltpu.SemaphoreType.DMA
    return pl.pallas_call(
        functools.partial(experts_kernel, n_sp, n_tp, lag, cap, top),
        out_shape=jax.ShapeDtypeStruct((rows, width), bf),
        in_specs=[anywhere] * 3 + [vmem] * 6 + [anywhere] * 7,
        out_specs=vmem,
        scratch_shapes=[
            pltpu.VMEM((length, channels), bf),
            pltpu.VMEM((length + HALO, channels), bf),
            pltpu.VMEM((length + HALO, channels), bf),
            pltpu.VMEM((n_tp, rows, channels), bf),
            pltpu.VMEM((n_tp, rows, channels), bf),
            pltpu.VMEM((n_sp, rows, width), bf),
            pltpu.VMEM((n_sp, META_ROWS, rows), f32),
            pltpu.VMEM((n_sp, group, width), bf),
            pltpu.VMEM((2, n_sp * wide * cap, width), bf),
            pltpu.VMEM((2, n_sp * wide * cap, width), bf),
            pltpu.VMEM((n_sp, group, width), bf),
            pltpu.VMEM((half, rows, width), bf),
            pltpu.VMEM((half, rows, width), bf),
            pltpu.VMEM((rows, width), f32),
            pltpu.VMEM((n_tp * channels, width), bf),
            pltpu.VMEM((width, hidden), bf),
            pltpu.VMEM((width, hidden), bf),
            pltpu.VMEM((hidden, width), bf),
            pltpu.VMEM((width, shared_hidden), bf),
            pltpu.VMEM((width, shared_hidden), bf),
            pltpu.VMEM((shared_hidden, width), bf),
            dma((10,)),
            dma((2,)),
            dma((2,)),
            dma((n_tp,)),
            dma((n_tp,)),
            dma((n_sp,)),
            dma((n_sp,)),
            dma((2, half, 2)),
            dma((2, half, 2)),
            dma((n_sp, n_tp)),
            dma((2, n_sp, wide)),
            dma((2, n_sp, wide)),
            dma((n_sp, n_tp)),
            dma((2, half + 1, 2)),
            dma((2, half + 1, 2)),
        ],
        compiler_params=pltpu.CompilerParams(
            collective_id=0, has_side_effects=True, vmem_limit_bytes=63 * 1024 * 1024
        ),
    )(
        out_gate, in_gate, conv_values, conv_taps, mix_gain.reshape(1, n_tp * channels),
        residual, ffn_gain.reshape(1, width), routes.T, route_weights.T,
        out_proj, expert_gate, expert_up, expert_down, shared_gate, shared_up, shared_down,
    )


def solution(mesh):
    in_specs = (
        P("sp", "tp"),
        P("sp", "tp"),
        P("sp", "tp"),
        P(None, "tp"),
        P(),
        P(),
        P(("sp", "tp"), None),
        P(),
        P(("sp", "tp"), None),
        P(("sp", "tp"), None),
        P(),
        P(),
        P(),
        P(("sp", "tp"), None, None),
        P(("sp", "tp"), None, None),
        P(("sp", "tp"), None, None),
    )
    out_specs = P(("sp", "tp"), None)
    return jax.shard_map(body, mesh=mesh, in_specs=in_specs, out_specs=out_specs, check_vma=False)
```

time: 135 us -> 124 us (0.919); the launches traced: 135 us -> 122 us
  Pallas kernels: 131 us -> 118 us
    pallas_call x1, Pallas kernels: 131 us -> 118 us  [body(): pl.pallas_call(functools.partial(experts_kernel, n_sp, n_tp, lag, cap, to...]
where the time goes in v1:
time: 124 us; the launch traced here: 122 us
  Pallas kernels  118 us (95%)
  local copies, waits for them, and re-layouts  3.18 us (3%)
    pallas_call x1, Pallas kernels, body(): pl.pallas_call(functools.partial(experts_kernel, n_sp, n_tp, lag, cap, to...  118 us

profile of v1, /device:TPU:0, one launch (start us, length us, event | category | flops | bytes accessed | tf_op | source)
XLA Modules:
  0.0 121.6 jit_solution(10317421966572798752)
XLA Ops:
  0.0 1.3 %reshape.6.mix_gain = f32[1,1536]{1,0:T(1,128)} reshape(f32[1536]{0:T(1024)} %param.20) | data formatting | bytes 12288 | tf_op jit(solution)/shard_map/reshape | solution.py:584
  1.3 118.4 %shard_map.154 = bf16[128,2048]{1,0:T(8,128)(2,1)} custom-call(bf16[512,384]{1,0:T(8,128)(2,1)} %og_hbm.1, bf16[512,384]{1,0:T(8,128)(2,1)} %ig_hbm.1, bf16[512,384]{1,0:T(8,128)(2,1)} %cv_hbm.1, f32[3,384]{1,0:T(4,128)} %taps.1, f32[1,1536]{1,0:T(1,128)} %reshape.6.mix_gain, bf16[128,2048]{1,0:T(8,128)(2,1)} %residual.1, f32[1,2048]{1,0:T(1,128)} %bitcast.3, ...), custom_call_target="tpu_custom_call" | custom-call | tf_op jit(solution)/shard_map/pallas_call | solution.py:537
  119.8 1.9 %copy.18 = bf16[128,2048]{1,0:T(8,128)(2,1)} copy(bf16[128,2048]{1,0:T(8,128)(2,1)} %shard_map.154) | data formatting | bytes 1048576

commit v2 on v1

--- a/solution.py
+++ b/solution.py
@@ -20,15 +20,16 @@
 
 
 def experts_kernel(
-    n_sp, n_tp, lag, cap, top,
-    og_hbm, ig_hbm, cv_hbm, taps, mix_gain, residual, ffn_gain, routes, route_weights,
-    op_hbm, eg_hbm, eu_hbm, ed_hbm, sg_hbm, su_hbm, sd_hbm,
+    n_sp, n_tp, cap, top,
+    og_hbm, ig_hbm, cv_hbm, taps_hbm, mix_gain_hbm, residual_hbm, ffn_gain_hbm,
+    routes_hbm, route_weights_hbm, op_hbm, eg_hbm, eu_hbm, ed_hbm, sg_hbm, su_hbm, sd_hbm,
     out,
+    taps, mix_gain, residual, ffn_gain, routes, route_weights, result,
     og, ig, cv, conv_out, conv_in,
     gathered, metas, staged, arrived, results, returned,
-    left_in, right_in, total,
+    left_in, right_in, total, parts,
     op, eg, eu, ed, sg, su, sd,
-    w_sem, halo_send, halo_recv, conv_send, conv_recv,
+    w_sem, small_sem, out_sem, halo_send, halo_recv, conv_send, conv_recv,
     meta_send, meta_recv, ring_send, ring_recv,
     disp_send, disp_recv, ret_send, ret_recv, red_send, red_recv,
 ):
@@ -79,8 +80,8 @@
     def greet(device):
         pl.semaphore_signal(barrier, inc=1, device_id=device, device_id_type=MESH)
 
-    for d in range(1, n_sp):
-        greet(ahead(d))
+    greet(right)
+    greet(left)
     for j in range(1, n_tp):
         greet((sp, lax.rem(tp + j, n_tp)))
         greet(device_at(1, z * wide + y, lax.rem(x * 2 + core + j, n_tp)))
@@ -95,7 +96,14 @@
              (eg_hbm.at[0], eg), (eu_hbm.at[0], eu), (ed_hbm.at[0], ed))
         )
     ]
-    for copy in weights[:4]:
+    smalls = [
+        pltpu.make_async_copy(src, dst, small_sem.at[i])
+        for i, (src, dst) in enumerate(
+            ((taps_hbm, taps), (routes_hbm, routes), (route_weights_hbm, route_weights),
+             (mix_gain_hbm, mix_gain), (ffn_gain_hbm, ffn_gain), (residual_hbm, residual))
+        )
+    ]
+    for copy in weights[:2] + smalls[:1] + weights[2:3] + smalls[1:] + weights[3:4]:
         copy.start()
 
     def remote(src, dst, send, recv, device):
@@ -104,8 +112,11 @@
             device_id=device, device_id_type=MESH,
         )
 
-    def meta_copy(d):
-        return remote(metas.at[0], metas.at[d], meta_send.at[d], meta_recv.at[d], ahead(d))
+    def meta_copy(s, way):
+        dst = metas.at[s + 1 if way == 0 else n_sp - s - 1]
+        src = metas.at[s if way == 0 else lax.rem(n_sp - s, n_sp)]
+        device = right if way == 0 else left
+        return remote(src, dst, meta_send.at[way, s], meta_recv.at[way, s], device)
 
     def part_of(h):
         return pl.ds(h * mid, mid)
@@ -119,10 +130,13 @@
     def slots(index):
         return pl.ds(pl.multiple_of(index * cap, cap), cap)
 
+    def row_of(kind, p, b):
+        return slots((p * 2 + kind) * wide + b)
+
     def disp_copy(p, j):
         to = lax.rem(member + j, n_tp)
         return remote(
-            staged.at[p, slots(to)], arrived.at[core, slots(p * wide + across(core))],
+            staged.at[p, slots(to)], arrived.at[row_of(core, p, across(core))],
             disp_send.at[p, j], disp_recv.at[core, p, across(core)], device_at(core, ring, to),
         )
 
@@ -134,21 +148,21 @@
 
     def disp_arrival(kind, p, b):
         return remote(
-            staged.at[p, slots(0)], arrived.at[kind, slots(p * wide + b)],
+            staged.at[p, slots(0)], arrived.at[row_of(kind, p, b)],
             disp_send.at[p, 0], disp_recv.at[kind, p, b], holder(kind, b),
         )
 
     def ret_copy(kind, p, b):
         me = across(kind) * 2 + core
         return remote(
-            results.at[kind, slots(p * wide + b)], returned.at[p, slots(me)],
+            results.at[row_of(kind, p, b)], returned.at[p, slots(me)],
             ret_send.at[kind, p, b], ret_recv.at[p, me], holder(kind, b),
         )
 
     def ret_arrival(p, j):
         frm = lax.rem(member + j, n_tp)
         return remote(
-            results.at[0, slots(0)], returned.at[p, slots(frm)],
+            results.at[slots(0)], returned.at[p, slots(frm)],
             ret_send.at[0, p, 0], ret_recv.at[p, frm], device_at(core, ring, frm),
         )
 
@@ -166,13 +180,59 @@
             halo_send.at[i], halo_recv.at[i], device,
         )
 
-    def conv_copy(t):
+    pieces = (pl.ds(0, HALO), pl.ds(HALO, rows - HALO))
+
+    def conv_copy(t, i):
         return remote(
-            conv_out.at[t], conv_in.at[tp], conv_send.at[t], conv_recv.at[tp], (sp, t)
-        )
-
-    def conv_arrival(t):
-        return remote(conv_out.at[t], conv_in.at[t], conv_send.at[t], conv_recv.at[t], (sp, t))
+            conv_out.at[t, pieces[i]], conv_in.at[tp, pieces[i]],
+            conv_send.at[t, i], conv_recv.at[tp, i], (sp, t),
+        )
+
+    def conv_arrival(t, i):
+        return remote(
+            conv_out.at[t, pieces[i]], conv_in.at[t, pieces[i]],
+            conv_send.at[t, i], conv_recv.at[t, i], (sp, t),
+        )
+
+    taps_count = taps.shape[0]
+
+    def convolve(t, first, count):
+        span = pl.ds(t * rows + first, count + HALO)
+        mixed = ig[span].astype(jnp.float32) * cv[span].astype(jnp.float32)
+        if t == 0 and first == 0:
+            blank = jnp.where(sp == 0, HALO, 0)
+            at = lax.broadcasted_iota(jnp.int32, mixed.shape, 0)
+            mixed = jnp.where(at >= blank, mixed, 0.0)
+        base = HALO - (taps_count - 1)
+        filtered = taps[0:1, :] * mixed[base : base + count]
+        for o in range(1, taps_count):
+            filtered = filtered + taps[o : o + 1, :] * mixed[base + o : base + o + count]
+        gate = og[pl.ds(t * rows + first, count)].astype(jnp.float32)
+        conv_out[t, pl.ds(first, count)] = (gate * filtered).astype(jnp.bfloat16)
+
+    def send_conv(t, some):
+        @pl.when(tp != t)
+        def _():
+            for i in some:
+                conv_copy(t, i).start()
+
+    owners = [t for t in range(2, n_tp, 2)] + [t for t in range(1, n_tp, 2)]
+    for copy in weights[:3] + smalls[:1]:
+        copy.wait()
+    for t in owners:
+        convolve(t, 0, rows)
+    convolve(0, HALO, rows - HALO)
+    with jax.named_scope("barrier"):
+        pl.semaphore_wait(barrier, 2 + 2 * (n_tp - 1) + 2)
+    halo_copy(0).start()
+    halo_copy(1).start()
+    for t in owners:
+        send_conv(t, (1, 0))
+    send_conv(0, (1,))
+    for copy in weights[4:7]:
+        copy.start()
+    for copy in smalls[1:]:
+        copy.wait()
 
     experts_total = n_sp * n_tp
     expert = lax.broadcasted_iota(jnp.int32, (experts_total, rows), 0)
@@ -205,41 +265,11 @@
     weight = route_weights[...]
     metas[0, top : 2 * top, :] = weight / jnp.sum(weight, axis=0, keepdims=True) * 2.5
 
-    for copy in weights[:3]:
-        copy.wait()
-    with jax.named_scope("barrier"):
-        pl.semaphore_wait(barrier, n_sp - 1 + 2 * (n_tp - 1) + 2)
-    halo_copy(0).start()
-    halo_copy(1).start()
-    for copy in weights[4:7]:
-        copy.start()
-
-    taps_count = taps.shape[0]
-    owners = [t for t in range(2, n_tp, 2)] + [t for t in range(1, n_tp, 2)] + [0]
-    for t in owners:
-        if t == 0:
-            with jax.named_scope("halo_wait"):
-                halo_copy(0).wait_recv()
-                halo_copy(1).wait_recv()
-        span = pl.ds(t * rows, rows + HALO)
-        mixed = ig[span].astype(jnp.float32) * cv[span].astype(jnp.float32)
-        if t == 0:
-            blank = jnp.where(sp == 0, HALO, 0)
-            at = lax.broadcasted_iota(jnp.int32, mixed.shape, 0)
-            mixed = jnp.where(at >= blank, mixed, 0.0)
-        base = HALO - (taps_count - 1)
-        filtered = taps[0:1, :] * mixed[base : base + rows]
-        for o in range(1, taps_count):
-            filtered = filtered + taps[o : o + 1, :] * mixed[base + o : base + o + rows]
-        value = (og[pl.ds(t * rows, rows)].astype(jnp.float32) * filtered).astype(jnp.bfloat16)
-        conv_out[t] = value
-
-        @pl.when(tp != t)
-        def _():
-            conv_copy(t).start()
-
-    for d in range(1, n_sp):
-        meta_copy(d).start()
+    with jax.named_scope("halo_wait"):
+        halo_copy(0).wait_recv()
+        halo_copy(1).wait_recv()
+    convolve(0, 0, HALO)
+    send_conv(0, (0,))
     weights[3].wait()
     for copy in weights[7:]:
         copy.start()
@@ -247,6 +277,7 @@
     squares = jnp.zeros((rows, 1), jnp.float32)
     product = jnp.zeros((rows, width), jnp.float32)
     part_width = conv_in.shape[2]
+    gains = mix_gain[...].reshape(1, n_tp * part_width)
     sources = [tp, tp + 1 - 2 * core]
     for i in range(1, wide):
         other = lax.rem(y + i, wide) * 2
@@ -256,11 +287,12 @@
             value = conv_out[t].astype(jnp.float32)
         else:
             with jax.named_scope("conv_wait"):
-                conv_arrival(t).wait_recv()
+                for i in range(2):
+                    conv_arrival(t, i).wait_recv()
             value = conv_in[t].astype(jnp.float32)
-        gain = mix_gain[:, :part_width]
+        gain = gains[:, :part_width]
         for k in range(1, n_tp):
-            gain = jnp.where(t == k, mix_gain[:, k * part_width : (k + 1) * part_width], gain)
+            gain = jnp.where(t == k, gains[:, k * part_width : (k + 1) * part_width], gain)
         squares = squares + jnp.sum(value * value, axis=1, keepdims=True)
         product = product + jnp.dot(
             (value * gain).astype(jnp.bfloat16),
@@ -289,17 +321,30 @@
         ).astype(jnp.bfloat16)
         for j in range(1, n_tp):
             disp_copy(p, j).start()
-        arrived[core, slots(p * wide + across(core))] = staged[p, slots(member)]
+        arrived[row_of(core, p, across(core))] = staged[p, slots(member)]
 
     def gather_action(a):
         @pl.when(a == 0)
         def _():
             for h in range(2):
                 for way in range(2):
+                    if h == 0:
+                        meta_copy(0, way).start()
                     ring_copy(0, way, way if h == 0 else 1 - way).start()
 
         @pl.when(a > 0)
         def _():
+            meta_copy(a - 1, 0).wait_recv()
+
+            @pl.when(a < half)
+            def _():
+                meta_copy(a, 0).start()
+                meta_copy(a - 1, 1).wait_recv()
+
+            @pl.when(a < half - 1)
+            def _():
+                meta_copy(a, 1).start()
+
             for way in range(2):
                 with jax.named_scope("ring_wait"):
                     ring_copy(a - 1, way, way).wait_recv()
@@ -319,64 +364,39 @@
                         ring_copy(a, way, 1 - way).start()
 
         def one(i, c):
-            d = a + i * (n_sp - 2 * a)
-
-            @pl.when(d > 0)
-            def _():
-                meta_copy(d).wait_recv()
-
             with jax.named_scope("dispatch"):
-                dispatch(d, jnp.maximum(2 * a - 1, 0) + i)
+                dispatch(a + i * (n_sp - 2 * a), jnp.maximum(2 * a - 1, 0) + i)
             return c
 
         count = jnp.where(jnp.logical_or(a == 0, a == half), 1, 2)
         lax.fori_loop(0, count, one, 0)
 
-    def run_expert(kind, p, count):
+    def run_expert(p, count):
         with jax.named_scope("disp_wait"):
             for i in range(count):
-                for b in range(wide):
-                    @pl.when(jnp.logical_not(is_own(kind, b)))
-                    def _():
-                        disp_arrival(kind, p + i, b).wait_recv()
-
-        span = pl.ds(pl.multiple_of(p * batch, batch), count * batch)
+                for kind in range(2):
+                    for b in range(wide):
+
+                        @pl.when(jnp.logical_not(is_own(kind, b)))
+                        def _():
+                            disp_arrival(kind, p + i, b).wait_recv()
+
+        span = pl.ds(pl.multiple_of(p * 2 * batch, 2 * batch), count * 2 * batch)
         with jax.named_scope("ffn"):
-            results[kind, span] = ffn(arrived[kind, span], eg, eu, ed).astype(jnp.bfloat16)
-
-    def give_back(kind, p):
-        for b in range(wide):
-            own = is_own(kind, b)
-
-            @pl.when(jnp.logical_not(own))
-            def _():
-                ret_copy(kind, p, b).start()
-
-            @pl.when(own)
-            def _():
-                returned[p, slots(member)] = results[kind, slots(p * wide + b)]
-
-    def expert_action(kind, u):
-        @pl.when(jnp.logical_and(u > 1, u <= half))
-        def _():
-            run_expert(kind, 2 * u - 3, 2)
-
-        @pl.when(jnp.logical_or(u == 1, u == half))
-        def _():
-            run_expert(kind, jnp.where(u == 1, 0, n_sp - 1), 1)
-
-        @pl.when(u == half)
-        def _():
-            give_back(kind, n_sp - 1)
-
-        @pl.when(jnp.logical_and(u >= half, u <= 2 * half - 2))
-        def _():
-            give_back(kind, 4 * half - 3 - 2 * u)
-            give_back(kind, 4 * half - 2 - 2 * u)
-
-        @pl.when(u == 2 * half - 2)
-        def _():
-            give_back(kind, 0)
+            results[span] = ffn(arrived[span], eg, eu, ed).astype(jnp.bfloat16)
+
+    def give_back(p):
+        for kind in range(2):
+            for b in range(wide):
+                own = is_own(kind, b)
+
+                @pl.when(jnp.logical_not(own))
+                def _():
+                    ret_copy(kind, p, b).start()
+
+                @pl.when(own)
+                def _():
+                    returned[p, slots(member)] = results[row_of(kind, p, b)]
 
     def combine(d, p):
         with jax.named_scope("ret_wait"):
@@ -401,84 +421,101 @@
         red_copy(half, 1, 1).start()
 
     def reduce_step(s):
-        for way, buf_in in enumerate((left_in, right_in)):
-            d, p = (s, 2 * s - 1) if way == 0 else (n_sp - s, 2 * s)
-            part = combine(d, p)
-            for order in range(2):
-                h = way if order == 0 else 1 - way
-                if order == 0:
+        ways = ((s, 2 * s - 1, left_in), (n_sp - s, 2 * s, right_in))
+        for way, (d, p, _) in enumerate(ways):
+            parts[way] = combine(d, p)
+        for order in range(2):
+            for way, (d, _, buf_in) in enumerate(ways):
+                h = 1 - way if order == 0 else way
+                at = slice(h * mid, (h + 1) * mid)
+
+                def add():
                     with jax.named_scope("red_wait"):
                         red_copy(s + 1, way, h).wait_recv()
+                    gathered[d, at] = (parts[way, at] + buf_in[s, at].astype(jnp.float32)).astype(
+                        jnp.bfloat16
+                    )
+
+                if order == 0:
+                    pl.when(s < half - 1)(add)
+
+                    @pl.when(s == half - 1)
+                    def _():
+                        gathered[d, at] = parts[way, at].astype(jnp.bfloat16)
                 else:
-
-                    @pl.when(s < half - 1)
-                    def _():
-                        with jax.named_scope("red_wait2"):
-                            red_copy(s + 1, way, h).wait_recv()
-
-                at = slice(h * mid, (h + 1) * mid)
-                gathered[d, at] = (part[at] + buf_in[s, at].astype(jnp.float32)).astype(
-                    jnp.bfloat16
-                )
+                    add()
                 red_copy(s, way, h).start()
 
     def finish():
-        part = combine(0, 0) + total[...]
-        for way, buf_in in enumerate((left_in, right_in)):
-            with jax.named_scope("red_wait_last"):
-                for h in range(2):
-                    red_copy(1, way, h).wait_recv()
-            part = part + buf_in[0].astype(jnp.float32)
-        out[...] = part.astype(out.dtype)
-
-    left_in[half - 1, mid:] = jnp.zeros((rows - mid, width), jnp.bfloat16)
-    right_in[half - 1, :mid] = jnp.zeros((mid, width), jnp.bfloat16)
+        total[...] += combine(0, 0)
+        for order in range(2):
+            for way in range(2):
+                with jax.named_scope("red_wait_last"):
+                    red_copy(1, way, 1 - way if order == 0 else way).wait_recv()
+        result[...] = (
+            total[...] + left_in[0].astype(jnp.float32) + right_in[0].astype(jnp.float32)
+        ).astype(result.dtype)
 
     def step(k, carry):
-        a = k - lag * core
-
-        @pl.when(jnp.logical_and(a >= 0, a <= half))
-        def _():
-            gather_action(a)
-
-        @pl.when(k == 0)
-        def _():
+        @pl.when(k <= half)
+        def _():
+            gather_action(k)
+
+        @pl.when(k == 1)
+        def _():
+            for copy in weights[7:]:
+                copy.wait()
+
+        @pl.when(jnp.logical_and(k > 1, k <= half))
+        def _():
+            run_expert(2 * k - 3, 2)
+
+        @pl.when(jnp.logical_or(k == 1, k == half))
+        def _():
+            run_expert(jnp.where(k == 1, 0, n_sp - 1), 1)
+
+        @pl.when(k == half)
+        def _():
+            give_back(n_sp - 1)
             for copy in weights[4:7]:
                 copy.wait()
             with jax.named_scope("shared"):
                 total[...] += ffn(gathered[0], sg, su, sd)
-            for copy in weights[7:]:
-                copy.wait()
-
-        def kinds(kind, c):
-            expert_action(kind, k - lag * kind)
-            return c
-
-        lax.fori_loop(0, 2, kinds, 0)
-
-        @pl.when(a == half + 1)
+
+        @pl.when(k == half + 1)
         def _():
             reduce_start()
 
-        @pl.when(jnp.logical_and(a > half + 1, a <= 2 * half))
-        def _():
-            reduce_step(2 * half + 1 - a)
-
-        @pl.when(a == 2 * half + 1)
-        def _():
-            finish()
+        @pl.when(k > half + 1)
+        def _():
+            reduce_step(2 * half + 1 - k)
+
+        @pl.when(jnp.logical_and(k >= half, k <= 2 * half - 2))
+        def _():
+            give_back(4 * half - 3 - 2 * k)
+            give_back(4 * half - 2 - 2 * k)
+
+        @pl.when(k == 2 * half - 2)
+        def _():
+            give_back(0)
 
         return carry
 
-    lax.fori_loop(0, lag + 2 * half + 2, step, 0)
-
-    for d in range(1, n_sp):
-        meta_copy(d).wait_send()
+    lax.fori_loop(0, 2 * half + 1, step, 0)
+    finish()
+    write = pltpu.make_async_copy(result, out, out_sem)
+    write.start()
+
+    for s in range(half):
+        meta_copy(s, 0).wait_send()
+        if s < half - 1:
+            meta_copy(s, 1).wait_send()
     for t in range(n_tp):
 
         @pl.when(tp != t)
         def _():
-            conv_copy(t).wait_send()
+            for i in range(2):
+                conv_copy(t, i).wait_send()
 
     for way in range(2):
         halo_copy(way).wait_send()
@@ -500,6 +537,7 @@
         return c
 
     lax.fori_loop(0, n_sp, drain, 0)
+    write.wait()
 
 
 def body(
@@ -529,17 +567,22 @@
     half = n_sp // 2
     group = n_tp * cap
     wide = n_tp // 2
-    lag = 0
     bf, f32 = jnp.bfloat16, jnp.float32
-    vmem = pl.BlockSpec(memory_space=pltpu.VMEM)
     anywhere = pl.BlockSpec(memory_space=pl.ANY)
     dma = pltpu.SemaphoreType.DMA
     return pl.pallas_call(
-        functools.partial(experts_kernel, n_sp, n_tp, lag, cap, top),
+        functools.partial(experts_kernel, n_sp, n_tp, cap, top),
         out_shape=jax.ShapeDtypeStruct((rows, width), bf),
-        in_specs=[anywhere] * 3 + [vmem] * 6 + [anywhere] * 7,
-        out_specs=vmem,
+        in_specs=[anywhere] * 16,
+        out_specs=anywhere,
         scratch_shapes=[
+            pltpu.VMEM(conv_taps.shape, f32),
+            pltpu.VMEM(mix_gain.shape, f32),
+            pltpu.VMEM((rows, width), bf),
+            pltpu.VMEM((1, width), f32),
+            pltpu.VMEM((top, rows), jnp.int32),
+            pltpu.VMEM((top, rows), f32),
+            pltpu.VMEM((rows, width), bf),
             pltpu.VMEM((length, channels), bf),
             pltpu.VMEM((length + HALO, channels), bf),
             pltpu.VMEM((length + HALO, channels), bf),
@@ -548,12 +591,13 @@
             pltpu.VMEM((n_sp, rows, width), bf),
             pltpu.VMEM((n_sp, META_ROWS, rows), f32),
             pltpu.VMEM((n_sp, group, width), bf),
-            pltpu.VMEM((2, n_sp * wide * cap, width), bf),
-            pltpu.VMEM((2, n_sp * wide * cap, width), bf),
+            pltpu.VMEM((n_sp * group, width), bf),
+            pltpu.VMEM((n_sp * group, width), bf),
             pltpu.VMEM((n_sp, group, width), bf),
             pltpu.VMEM((half, rows, width), bf),
             pltpu.VMEM((half, rows, width), bf),
             pltpu.VMEM((rows, width), f32),
+            pltpu.VMEM((2, rows, width), f32),
             pltpu.VMEM((n_tp * channels, width), bf),
             pltpu.VMEM((width, hidden), bf),
             pltpu.VMEM((width, hidden), bf),
@@ -562,12 +606,14 @@
             pltpu.VMEM((width, shared_hidden), bf),
             pltpu.VMEM((shared_hidden, width), bf),
             dma((10,)),
+            dma((6,)),
+            dma(()),
             dma((2,)),
             dma((2,)),
-            dma((n_tp,)),
-            dma((n_tp,)),
-            dma((n_sp,)),
-            dma((n_sp,)),
+            dma((n_tp, 2)),
+            dma((n_tp, 2)),
+            dma((2, half)),
+            dma((2, half)),
             dma((2, half, 2)),
             dma((2, half, 2)),
             dma((n_sp, n_tp)),
@@ -581,7 +627,7 @@
             collective_id=0, has_side_effects=True, vmem_limit_bytes=63 * 1024 * 1024
         ),
     )(
-        out_gate, in_gate, conv_values, conv_taps, mix_gain.reshape(1, n_tp * channels),
+        out_gate, in_gate, conv_values, conv_taps, mix_gain,
         residual, ffn_gain.reshape(1, width), routes.T, route_weights.T,
         out_proj, expert_gate, expert_up, expert_down, shared_gate, shared_up, shared_down,
     )

time: 124 us -> 112 us (0.903); the launches traced: 122 us -> 112 us
  Pallas kernels: 118 us -> 110 us
  local copies, waits for them, and re-layouts: 3.18 us -> 1.88 us
    pallas_call x1, Pallas kernels: 118 us -> 110 us  [body(): pl.pallas_call(functools.partial(experts_kernel, n_sp, n_tp, cap, top), o...]
    reshape x1 -> x0, local copies, waits for them, and re-layouts: 1.29 us -> none  [body(): mix_gain.reshape(1, n_tp * channels)]
where the time goes in v2:
time: 112 us
  Pallas kernels  110 us (98%)
  local copies, waits for them, and re-layouts  1.88 us (2%)
    pallas_call x1, Pallas kernels, body(): pl.pallas_call(functools.partial(experts_kernel, n_sp, n_tp, cap, top), o...  110 us

profile of v2, /device:TPU:0, one launch (start us, length us, event | category | flops | bytes accessed | tf_op | source)
XLA Modules:
  0.0 112.0 jit_solution(12325839140559097639)
XLA Ops:
  0.0 110.1 %shard_map.154 = bf16[128,2048]{1,0:T(8,128)(2,1)} custom-call(bf16[512,384]{1,0:T(8,128)(2,1)} %og_hbm.1, bf16[512,384]{1,0:T(8,128)(2,1)} %ig_hbm.1, bf16[512,384]{1,0:T(8,128)(2,1)} %cv_hbm.1, f32[3,384]{1,0:T(4,128)} %taps_hbm.1, f32[1536]{0:T(1024)} %mix_gain_hbm.1, bf16[128,2048]{1,0:T(8,128)(2,1)} %residual_hbm.1, f32[1,2048]{1,0:T(1,128)} %bitcast.3, ...), custom_call_target="tpu_custom_call" | custom-call | tf_op jit(solution)/shard_map/pallas_call | solution.py:573
  110.1 1.9 %copy.18 = bf16[128,2048]{1,0:T(8,128)(2,1)} copy(bf16[128,2048]{1,0:T(8,128)(2,1)} %shard_map.154) | data formatting | bytes 1048576

commit v3 on v2

--- a/solution.py
+++ b/solution.py
@@ -24,12 +24,12 @@
     og_hbm, ig_hbm, cv_hbm, taps_hbm, mix_gain_hbm, residual_hbm, ffn_gain_hbm,
     routes_hbm, route_weights_hbm, op_hbm, eg_hbm, eu_hbm, ed_hbm, sg_hbm, su_hbm, sd_hbm,
     out,
-    taps, mix_gain, residual, ffn_gain, routes, route_weights, result,
+    taps, mix_gain, residual, ffn_gain, routes, route_weights,
     og, ig, cv, conv_out, conv_in,
     gathered, metas, staged, arrived, results, returned,
     left_in, right_in, total, parts,
     op, eg, eu, ed, sg, su, sd,
-    w_sem, small_sem, out_sem, halo_send, halo_recv, conv_send, conv_recv,
+    w_sem, small_sem, halo_send, halo_recv, conv_send, conv_recv,
     meta_send, meta_recv, ring_send, ring_recv,
     disp_send, disp_recv, ret_send, ret_recv, red_send, red_recv,
 ):
@@ -38,7 +38,7 @@
     half = n_sp // 2
     rows, width = total.shape
     length = og.shape[0]
-    mid = rows // 2
+    mid = width // 2
     group = n_tp * cap
     wide = n_tp // 2
     batch = wide * cap
@@ -114,18 +114,21 @@
 
     def meta_copy(s, way):
         dst = metas.at[s + 1 if way == 0 else n_sp - s - 1]
-        src = metas.at[s if way == 0 else lax.rem(n_sp - s, n_sp)]
+        src = metas.at[s if way == 0 else turned(s)]
         device = right if way == 0 else left
-        return remote(src, dst, meta_send.at[way, s], meta_recv.at[way, s], device)
+        return remote(src, dst, meta_send, meta_recv.at[way, s], device)
 
     def part_of(h):
         return pl.ds(h * mid, mid)
 
+    def turned(s):
+        return lax.rem(n_sp - s, n_sp)
+
     def ring_copy(s, way, h):
-        dst = gathered.at[s + 1 if way == 0 else n_sp - s - 1, part_of(h)]
-        src = gathered.at[s if way == 0 else lax.rem(n_sp - s, n_sp), part_of(h)]
+        dst = gathered.at[s + 1 if way == 0 else n_sp - s - 1, :, part_of(h)]
+        src = gathered.at[s if way == 0 else turned(s), :, part_of(h)]
         device = right if way == 0 else left
-        return remote(src, dst, ring_send.at[way, s, h], ring_recv.at[way, s, h], device)
+        return remote(src, dst, ring_send, ring_recv.at[way, s, h], device)
 
     def slots(index):
         return pl.ds(pl.multiple_of(index * cap, cap), cap)
@@ -133,11 +136,13 @@
     def row_of(kind, p, b):
         return slots((p * 2 + kind) * wide + b)
 
-    def disp_copy(p, j):
+    def disp_copy(p, j, h):
         to = lax.rem(member + j, n_tp)
         return remote(
-            staged.at[p, slots(to)], arrived.at[row_of(core, p, across(core))],
-            disp_send.at[p, j], disp_recv.at[core, p, across(core)], device_at(core, ring, to),
+            staged.at[p, slots(to), part_of(h)],
+            arrived.at[row_of(core, p, across(core)), part_of(h)],
+            disp_send, disp_recv.at[p],
+            device_at(core, ring, to),
         )
 
     def is_own(kind, b):
@@ -146,38 +151,40 @@
     def holder(kind, b):
         return device_at(kind, z * wide + along(kind), b * 2 + kind)
 
-    def disp_arrival(kind, p, b):
+    others = pl.ds(0, (n_tp - 1) * cap)
+    blocks = pl.ds(0, n_sp * (n_tp - 1) // n_tp)
+    peers = pl.ds(0, n_sp - 1)
+
+    def disp_arrival(p):
         return remote(
-            staged.at[p, slots(0)], arrived.at[row_of(kind, p, b)],
-            disp_send.at[p, 0], disp_recv.at[kind, p, b], holder(kind, b),
-        )
-
-    def ret_copy(kind, p, b):
+            staged.at[p, others], arrived.at[others], disp_send, disp_recv.at[p], right
+        )
+
+    def ret_copy(kind, p, b, h):
         me = across(kind) * 2 + core
         return remote(
-            results.at[row_of(kind, p, b)], returned.at[p, slots(me)],
-            ret_send.at[kind, p, b], ret_recv.at[p, me], holder(kind, b),
-        )
-
-    def ret_arrival(p, j):
-        frm = lax.rem(member + j, n_tp)
+            results.at[row_of(kind, p, b), part_of(h)], returned.at[p, slots(me), part_of(h)],
+            ret_send, ret_recv.at[p, h], holder(kind, b),
+        )
+
+    def ret_arrival(p, h):
         return remote(
-            results.at[slots(0)], returned.at[p, slots(frm)],
-            ret_send.at[0, p, 0], ret_recv.at[p, frm], device_at(core, ring, frm),
+            results.at[others, part_of(h)], returned.at[p, others, part_of(h)],
+            ret_send, ret_recv.at[p, h], right,
         )
 
     def red_copy(s, way, h):
         device = left if way == 0 else right
-        src = gathered.at[s if way == 0 else n_sp - s, part_of(h)]
-        dst = (left_in if way == 0 else right_in).at[s - 1, part_of(h)]
-        return remote(src, dst, red_send.at[way, s, h], red_recv.at[way, s - 1, h], device)
+        src = gathered.at[s if way == 0 else n_sp - s, :, part_of(h)]
+        dst = (left_in if way == 0 else right_in).at[s - 1, :, part_of(h)]
+        return remote(src, dst, red_send, red_recv.at[way, s - 1, h], device)
 
     def halo_copy(i):
         buf = (ig, cv)[i]
         device = (lax.rem(sp + 1, n_sp), tp)
         return remote(
             buf.at[pl.ds(length, HALO)], buf.at[pl.ds(0, HALO)],
-            halo_send.at[i], halo_recv.at[i], device,
+            halo_send, halo_recv.at[i], device,
         )
 
     pieces = (pl.ds(0, HALO), pl.ds(HALO, rows - HALO))
@@ -185,14 +192,11 @@
     def conv_copy(t, i):
         return remote(
             conv_out.at[t, pieces[i]], conv_in.at[tp, pieces[i]],
-            conv_send.at[t, i], conv_recv.at[tp, i], (sp, t),
-        )
-
-    def conv_arrival(t, i):
-        return remote(
-            conv_out.at[t, pieces[i]], conv_in.at[t, pieces[i]],
-            conv_send.at[t, i], conv_recv.at[t, i], (sp, t),
-        )
+            conv_send, conv_recv.at[tp], (sp, t),
+        )
+
+    def conv_arrival(t):
+        return remote(conv_out.at[t], conv_in.at[t], conv_send, conv_recv.at[t], (sp, t))
 
     taps_count = taps.shape[0]
 
@@ -287,8 +291,7 @@
             value = conv_out[t].astype(jnp.float32)
         else:
             with jax.named_scope("conv_wait"):
-                for i in range(2):
-                    conv_arrival(t, i).wait_recv()
+                conv_arrival(t).wait_recv()
             value = conv_in[t].astype(jnp.float32)
         gain = gains[:, :part_width]
         for k in range(1, n_tp):
@@ -311,17 +314,18 @@
         at = lax.broadcasted_iota(jnp.int32, (group, rows), 0).astype(jnp.float32) + first_slot
         return at == meta[k : k + 1, :]
 
-    def dispatch(d, p):
+    def dispatch(d, p, h):
         meta = metas[d]
         pick = jnp.zeros((group, rows), jnp.float32)
         for k in range(top):
             pick = jnp.where(matches(meta, k), 1.0, pick)
-        staged[p] = jnp.dot(
-            pick.astype(jnp.bfloat16), gathered[d], preferred_element_type=jnp.float32
+        staged[p, :, part_of(h)] = jnp.dot(
+            pick.astype(jnp.bfloat16), gathered[d, :, part_of(h)],
+            preferred_element_type=jnp.float32,
         ).astype(jnp.bfloat16)
         for j in range(1, n_tp):
-            disp_copy(p, j).start()
-        arrived[row_of(core, p, across(core))] = staged[p, slots(member)]
+            disp_copy(p, j, h).start()
+        arrived[row_of(core, p, across(core)), part_of(h)] = staged[p, slots(member), part_of(h)]
 
     def gather_action(a):
         @pl.when(a == 0)
@@ -353,191 +357,164 @@
                 def _():
                     ring_copy(a, way, way).start()
 
-            @pl.when(a < half)
-            def _():
-                for way in range(2):
-                    with jax.named_scope("ring_wait"):
-                        ring_copy(a - 1, way, 1 - way).wait_recv()
-
-                    @pl.when(a < half - 1)
-                    def _():
-                        ring_copy(a, way, 1 - way).start()
-
-        def one(i, c):
+        alone = jnp.logical_or(a == 0, a == half)
+        low = jnp.maximum(2 * a - 1, 0)
+        ways = ((a, low), (turned(a), jnp.where(alone, low, 2 * a)))
+        for way, (d, p) in enumerate(ways):
             with jax.named_scope("dispatch"):
-                dispatch(a + i * (n_sp - 2 * a), jnp.maximum(2 * a - 1, 0) + i)
-            return c
-
-        count = jnp.where(jnp.logical_or(a == 0, a == half), 1, 2)
-        lax.fori_loop(0, count, one, 0)
+                dispatch(d, p, way)
+
+        @pl.when(jnp.logical_not(alone))
+        def _():
+            for way in range(2):
+                with jax.named_scope("ring_wait"):
+                    ring_copy(a - 1, way, 1 - way).wait_recv()
+
+                @pl.when(a < half - 1)
+                def _():
+                    ring_copy(a, way, 1 - way).start()
+
+            for way, (d, p) in enumerate(ways):
+                with jax.named_scope("dispatch"):
+                    dispatch(d, p, 1 - way)
 
     def run_expert(p, count):
         with jax.named_scope("disp_wait"):
             for i in range(count):
-                for kind in range(2):
-                    for b in range(wide):
-
-                        @pl.when(jnp.logical_not(is_own(kind, b)))
-                        def _():
-                            disp_arrival(kind, p + i, b).wait_recv()
+                disp_arrival(p + i).wait_recv()
 
         span = pl.ds(pl.multiple_of(p * 2 * batch, 2 * batch), count * 2 * batch)
         with jax.named_scope("ffn"):
             results[span] = ffn(arrived[span], eg, eu, ed).astype(jnp.bfloat16)
 
-    def give_back(p):
+    def give_back(p, h):
         for kind in range(2):
             for b in range(wide):
                 own = is_own(kind, b)
 
                 @pl.when(jnp.logical_not(own))
                 def _():
-                    ret_copy(kind, p, b).start()
+                    ret_copy(kind, p, b, h).start()
 
                 @pl.when(own)
                 def _():
-                    returned[p, slots(member)] = results[row_of(kind, p, b)]
-
-    def combine(d, p):
+                    returned[p, slots(member), part_of(h)] = results[
+                        row_of(kind, p, b), part_of(h)
+                    ]
+
+    def combine(d, p, h):
         with jax.named_scope("ret_wait"):
-            for j in range(1, n_tp):
-                ret_arrival(p, j).wait_recv()
+            ret_arrival(p, h).wait_recv()
         meta = metas[d]
         mix = jnp.zeros((group, rows), jnp.float32)
         for k in range(top):
             mix = jnp.where(matches(meta, k), meta[top + k : top + k + 1, :], mix)
         return lax.dot_general(
-            mix.astype(jnp.bfloat16), returned[p], (((0,), (0,)), ((), ())),
+            mix.astype(jnp.bfloat16), returned[p, :, part_of(h)], (((0,), (0,)), ((), ())),
             preferred_element_type=jnp.float32,
         )
 
-    def reduce_start():
-        for way in range(2):
-            for h in range(2):
-                for s in range(half - 1 if h != way else half):
-                    ring_copy(s, way, h).wait_send()
-        gathered[half] = combine(half, n_sp - 1).astype(jnp.bfloat16)
-        red_copy(half, 0, 0).start()
-        red_copy(half, 1, 1).start()
-
-    def reduce_step(s):
-        ways = ((s, 2 * s - 1, left_in), (n_sp - s, 2 * s, right_in))
-        for way, (d, p, _) in enumerate(ways):
-            parts[way] = combine(d, p)
-        for order in range(2):
-            for way, (d, _, buf_in) in enumerate(ways):
-                h = 1 - way if order == 0 else way
-                at = slice(h * mid, (h + 1) * mid)
-
-                def add():
-                    with jax.named_scope("red_wait"):
-                        red_copy(s + 1, way, h).wait_recv()
-                    gathered[d, at] = (parts[way, at] + buf_in[s, at].astype(jnp.float32)).astype(
-                        jnp.bfloat16
-                    )
-
-                if order == 0:
-                    pl.when(s < half - 1)(add)
-
-                    @pl.when(s == half - 1)
-                    def _():
-                        gathered[d, at] = parts[way, at].astype(jnp.bfloat16)
-                else:
-                    add()
-                red_copy(s, way, h).start()
-
-    def finish():
-        total[...] += combine(0, 0)
-        for order in range(2):
-            for way in range(2):
-                with jax.named_scope("red_wait_last"):
-                    red_copy(1, way, 1 - way if order == 0 else way).wait_recv()
-        result[...] = (
-            total[...] + left_in[0].astype(jnp.float32) + right_in[0].astype(jnp.float32)
-        ).astype(result.dtype)
-
-    def step(k, carry):
-        @pl.when(k <= half)
-        def _():
-            gather_action(k)
-
-        @pl.when(k == 1)
-        def _():
-            for copy in weights[7:]:
-                copy.wait()
-
-        @pl.when(jnp.logical_and(k > 1, k <= half))
-        def _():
-            run_expert(2 * k - 3, 2)
-
-        @pl.when(jnp.logical_or(k == 1, k == half))
-        def _():
-            run_expert(jnp.where(k == 1, 0, n_sp - 1), 1)
-
-        @pl.when(k == half)
-        def _():
-            give_back(n_sp - 1)
+    def reduce_part(s, late, first):
+        for way, buf_in in enumerate((left_in, right_in)):
+            h = way if late else 1 - way
+            d = s if way == 0 else n_sp - s
+            p = jnp.minimum(2 * s - 1 + way, n_sp - 1)
+            parts[way] = combine(d, p, h)
+        for way, buf_in in enumerate((left_in, right_in)):
+            h = way if late else 1 - way
+            d = s if way == 0 else n_sp - s
+
+            @pl.when(jnp.logical_not(first))
+            def _():
+                with jax.named_scope("red_wait"):
+                    red_copy(s + 1, way, h).wait_recv()
+                gathered[d, :, part_of(h)] = (
+                    parts[way] + buf_in[s, :, part_of(h)].astype(jnp.float32)
+                ).astype(jnp.bfloat16)
+
+            @pl.when(first)
+            def _():
+                gathered[d, :, part_of(h)] = parts[way].astype(jnp.bfloat16)
+
+            red_copy(s, way, h).start()
+
+    def gather_step(k, carry):
+        gather_action(k)
+
+        @pl.when(k == 0)
+        def _():
             for copy in weights[4:7]:
                 copy.wait()
             with jax.named_scope("shared"):
                 total[...] += ffn(gathered[0], sg, su, sd)
-
-        @pl.when(k == half + 1)
-        def _():
-            reduce_start()
-
-        @pl.when(k > half + 1)
-        def _():
-            reduce_step(2 * half + 1 - k)
-
-        @pl.when(jnp.logical_and(k >= half, k <= 2 * half - 2))
-        def _():
-            give_back(4 * half - 3 - 2 * k)
-            give_back(4 * half - 2 - 2 * k)
-
-        @pl.when(k == 2 * half - 2)
-        def _():
-            give_back(0)
+            for copy in weights[7:]:
+                copy.wait()
+
+        @pl.when(k > 1)
+        def _():
+            run_expert(2 * k - 3, 2)
+
+        @pl.when(k == half - 1)
+        def _():
+            give_back(0, 0)
+            give_back(0, 1)
+
+        @pl.when(k == half)
+        def _():
+            give_back(n_sp - 3, 1)
+            give_back(n_sp - 2, 0)
+
+        @pl.when(jnp.logical_or(k == 1, k == half))
+        def _():
+            run_expert(jnp.where(k == 1, 0, n_sp - 1), 1)
 
         return carry
 
-    lax.fori_loop(0, 2 * half + 1, step, 0)
-    finish()
-    write = pltpu.make_async_copy(result, out, out_sem)
-    write.start()
-
-    for s in range(half):
-        meta_copy(s, 0).wait_send()
-        if s < half - 1:
-            meta_copy(s, 1).wait_send()
-    for t in range(n_tp):
-
-        @pl.when(tp != t)
-        def _():
-            for i in range(2):
-                conv_copy(t, i).wait_send()
-
-    for way in range(2):
-        halo_copy(way).wait_send()
-        red_copy(half, way, way).wait_send()
-        for s in range(1, half):
+    lax.fori_loop(0, half + 1, gather_step, 0)
+    for h in range(2):
+        give_back(n_sp - 1, h)
+    remote(gathered.at[peers], gathered.at[peers], ring_send, ring_recv.at[0, 0, 0], right).wait_send()
+
+    def reduce_step(i, carry):
+        @pl.when(i < half - 1)
+        def _():
+            reduce_part(half - 1 - i, False, i == 0)
+
+        s = half - 1 - i
+
+        @pl.when(s > 1)
+        def _():
+            give_back(2 * s - 3, 1)
+            give_back(2 * s - 2, 0)
+
+        @pl.when(s > 0)
+        def _():
+            give_back(2 * s - 1, 0)
+            give_back(2 * s, 1)
+
+        reduce_part(half - i, True, i == 0)
+        return carry
+
+    lax.fori_loop(0, half, reduce_step, 0)
+    for h in range(2):
+        total[:, part_of(h)] += combine(0, 0, h)
+    with jax.named_scope("drain"):
+        for buf, part, sem in (
+            (metas, peers, meta_send), (conv_out, pl.ds(0, n_tp - 1), conv_send),
+            (conv_out, (0, pl.ds(0, 2 * HALO)), halo_send), (staged, blocks, disp_send),
+            (results, pl.ds(0, n_sp * (n_tp - 1) * cap), ret_send),
+        ):
+            remote(buf.at[part], buf.at[part], sem, halo_recv.at[0], right).wait_send()
+    with jax.named_scope("red_wait_last"):
+        for way in range(2):
             for h in range(2):
-                red_copy(s, way, h).wait_send()
-
-    def drain(p, c):
-        for j in range(1, n_tp):
-            disp_copy(p, j).wait_send()
-        for kind in range(2):
-            for b in range(wide):
-
-                @pl.when(jnp.logical_not(is_own(kind, b)))
-                def _():
-                    ret_copy(kind, p, b).wait_send()
-
-        return c
-
-    lax.fori_loop(0, n_sp, drain, 0)
-    write.wait()
+                red_copy(1, way, h).wait_recv()
+    out[...] = (
+        total[...] + left_in[0].astype(jnp.float32) + right_in[0].astype(jnp.float32)
+    ).astype(out.dtype)
+
+    with jax.named_scope("drain2"):
+        remote(gathered.at[peers], gathered.at[peers], red_send, halo_recv.at[0], right).wait_send()
 
 
 def body(
@@ -568,13 +545,12 @@
     group = n_tp * cap
     wide = n_tp // 2
     bf, f32 = jnp.bfloat16, jnp.float32
-    anywhere = pl.BlockSpec(memory_space=pl.ANY)
     dma = pltpu.SemaphoreType.DMA
     return pl.pallas_call(
         functools.partial(experts_kernel, n_sp, n_tp, cap, top),
-        out_shape=jax.ShapeDtypeStruct((rows, width), bf),
-        in_specs=[anywhere] * 16,
-        out_specs=anywhere,
+        out_shape=pltpu.VMEM((rows, width), bf),
+        in_specs=[pl.BlockSpec(memory_space=pltpu.HBM)] * 16,
+        out_specs=pl.BlockSpec(memory_space=pltpu.VMEM),
         scratch_shapes=[
             pltpu.VMEM(conv_taps.shape, f32),
             pltpu.VMEM(mix_gain.shape, f32),
@@ -582,7 +558,6 @@
             pltpu.VMEM((1, width), f32),
             pltpu.VMEM((top, rows), jnp.int32),
             pltpu.VMEM((top, rows), f32),
-            pltpu.VMEM((rows, width), bf),
             pltpu.VMEM((length, channels), bf),
             pltpu.VMEM((length + HALO, channels), bf),
             pltpu.VMEM((length + HALO, channels), bf),
@@ -597,7 +572,7 @@
             pltpu.VMEM((half, rows, width), bf),
             pltpu.VMEM((half, rows, width), bf),
             pltpu.VMEM((rows, width), f32),
-            pltpu.VMEM((2, rows, width), f32),
+            pltpu.VMEM((2, rows, width // 2), f32),
             pltpu.VMEM((n_tp * channels, width), bf),
             pltpu.VMEM((width, hidden), bf),
             pltpu.VMEM((width, hidden), bf),
@@ -609,22 +584,21 @@
             dma((6,)),
             dma(()),
             dma((2,)),
-            dma((2,)),
-            dma((n_tp, 2)),
-            dma((n_tp, 2)),
+            dma(()),
+            dma((n_tp,)),
+            dma(()),
             dma((2, half)),
-            dma((2, half)),
+            dma(()),
             dma((2, half, 2)),
+            dma(()),
+            dma((n_sp,)),
+            dma(()),
+            dma((n_sp, 2)),
+            dma(()),
             dma((2, half, 2)),
-            dma((n_sp, n_tp)),
-            dma((2, n_sp, wide)),
-            dma((2, n_sp, wide)),
-            dma((n_sp, n_tp)),
-            dma((2, half + 1, 2)),
-            dma((2, half + 1, 2)),
         ],
         compiler_params=pltpu.CompilerParams(
-            collective_id=0, has_side_effects=True, vmem_limit_bytes=63 * 1024 * 1024
+            collective_id=0, has_side_effects=True, vmem_limit_bytes=58 * 1024 * 1024
         ),
     )(
         out_gate, in_gate, conv_values, conv_taps, mix_gain,

time: 112 us -> 106 us (0.946)
  Pallas kernels: 110 us -> 105 us
    pallas_call x1, Pallas kernels: 110 us -> 105 us  [body(): pl.pallas_call(functools.partial(experts_kernel, n_sp, n_tp, cap, top), o...]
where the time goes in v3:
time: 106 us
  Pallas kernels  105 us (99%)
    pallas_call x1, Pallas kernels, body(): pl.pallas_call(functools.partial(experts_kernel, n_sp, n_tp, cap, top), o...  105 us

profile of v3, /device:TPU:0, one launch (start us, length us, event | category | flops | bytes accessed | tf_op | source)
XLA Modules:
  0.0 105.8 jit_solution(13775424521347112073)
XLA Ops:
  0.0 105.0 %shard_map.154 = bf16[128,2048]{1,0:T(8,128)(2,1)S(1)} custom-call(bf16[512,384]{1,0:T(8,128)(2,1)} %og_hbm.1, bf16[512,384]{1,0:T(8,128)(2,1)} %ig_hbm.1, bf16[512,384]{1,0:T(8,128)(2,1)} %cv_hbm.1, f32[3,384]{1,0:T(4,128)} %taps_hbm.1, f32[1536]{0:T(1024)} %mix_gain_hbm.1, bf16[128,2048]{1,0:T(8,128)(2,1)} %residual_hbm.1, f32[1,2048]{1,0:T(1,128)} %bitcast.3, ...), custom_call_target="tpu_custom_call" | custom-call | tf_op jit(solution)/shard_map/pallas_call | solution.py:549
  105.0 0.8 copy.18

commit v4 on v3

--- a/solution.py
+++ b/solution.py
@@ -85,8 +85,15 @@
     for j in range(1, n_tp):
         greet((sp, lax.rem(tp + j, n_tp)))
         greet(device_at(1, z * wide + y, lax.rem(x * 2 + core + j, n_tp)))
-    greet((lax.rem(sp + 1, n_sp), tp))
-    greet((lax.rem(sp + n_sp - 1, n_sp), tp))
+    has_next, has_last = sp < n_sp - 1, sp > 0
+
+    @pl.when(has_next)
+    def _():
+        greet((sp + 1, tp))
+
+    @pl.when(has_last)
+    def _():
+        greet((sp - 1, tp))
 
     weights = [
         pltpu.make_async_copy(src, dst, w_sem.at[i])
@@ -203,10 +210,6 @@
     def convolve(t, first, count):
         span = pl.ds(t * rows + first, count + HALO)
         mixed = ig[span].astype(jnp.float32) * cv[span].astype(jnp.float32)
-        if t == 0 and first == 0:
-            blank = jnp.where(sp == 0, HALO, 0)
-            at = lax.broadcasted_iota(jnp.int32, mixed.shape, 0)
-            mixed = jnp.where(at >= blank, mixed, 0.0)
         base = HALO - (taps_count - 1)
         filtered = taps[0:1, :] * mixed[base : base + count]
         for o in range(1, taps_count):
@@ -227,9 +230,14 @@
         convolve(t, 0, rows)
     convolve(0, HALO, rows - HALO)
     with jax.named_scope("barrier"):
-        pl.semaphore_wait(barrier, 2 + 2 * (n_tp - 1) + 2)
-    halo_copy(0).start()
-    halo_copy(1).start()
+        near = has_next.astype(jnp.int32) + has_last.astype(jnp.int32)
+        pl.semaphore_wait(barrier, 2 + 2 * (n_tp - 1) + near)
+
+    @pl.when(has_next)
+    def _():
+        halo_copy(0).start()
+        halo_copy(1).start()
+
     for t in owners:
         send_conv(t, (1, 0))
     send_conv(0, (1,))
@@ -269,9 +277,17 @@
     weight = route_weights[...]
     metas[0, top : 2 * top, :] = weight / jnp.sum(weight, axis=0, keepdims=True) * 2.5
 
-    with jax.named_scope("halo_wait"):
-        halo_copy(0).wait_recv()
-        halo_copy(1).wait_recv()
+    @pl.when(has_last)
+    def _():
+        with jax.named_scope("halo_wait"):
+            halo_copy(0).wait_recv()
+            halo_copy(1).wait_recv()
+
+    @pl.when(jnp.logical_not(has_last))
+    def _():
+        for buf in (ig, cv):
+            buf[pl.ds(0, HALO)] = jnp.zeros((HALO, buf.shape[1]), buf.dtype)
+
     convolve(0, 0, HALO)
     send_conv(0, (0,))
     weights[3].wait()
@@ -415,28 +431,27 @@
         )
 
     def reduce_part(s, late, first):
-        for way, buf_in in enumerate((left_in, right_in)):
+        for way in range(2):
             h = way if late else 1 - way
             d = s if way == 0 else n_sp - s
-            p = jnp.minimum(2 * s - 1 + way, n_sp - 1)
-            parts[way] = combine(d, p, h)
-        for way, buf_in in enumerate((left_in, right_in)):
-            h = way if late else 1 - way
-            d = s if way == 0 else n_sp - s
-
-            @pl.when(jnp.logical_not(first))
+            parts[way] = combine(d, jnp.minimum(2 * s - 1 + way, n_sp - 1), h)
+
+            @pl.when(first)
             def _():
+                gathered[d, :, part_of(h)] = parts[way].astype(jnp.bfloat16)
+                red_copy(s, way, h).start()
+
+        @pl.when(jnp.logical_not(first))
+        def _():
+            for way, buf_in in enumerate((left_in, right_in)):
+                h = way if late else 1 - way
+                d = s if way == 0 else n_sp - s
                 with jax.named_scope("red_wait"):
                     red_copy(s + 1, way, h).wait_recv()
                 gathered[d, :, part_of(h)] = (
                     parts[way] + buf_in[s, :, part_of(h)].astype(jnp.float32)
                 ).astype(jnp.bfloat16)
-
-            @pl.when(first)
-            def _():
-                gathered[d, :, part_of(h)] = parts[way].astype(jnp.bfloat16)
-
-            red_copy(s, way, h).start()
+                red_copy(s, way, h).start()
 
     def gather_step(k, carry):
         gather_action(k)
@@ -456,8 +471,8 @@
 
         @pl.when(k == half - 1)
         def _():
-            give_back(0, 0)
-            give_back(0, 1)
+            give_back(n_sp - 5, 1)
+            give_back(n_sp - 4, 0)
 
         @pl.when(k == half)
         def _():
@@ -482,7 +497,7 @@
 
         s = half - 1 - i
 
-        @pl.when(s > 1)
+        @pl.when(jnp.logical_and(s > 1, i > 0))
         def _():
             give_back(2 * s - 3, 1)
             give_back(2 * s - 2, 0)
@@ -491,6 +506,11 @@
         def _():
             give_back(2 * s - 1, 0)
             give_back(2 * s, 1)
+
+        @pl.when(s == 1)
+        def _():
+            give_back(0, 0)
+            give_back(0, 1)
 
         reduce_part(half - i, True, i == 0)
         return carry
@@ -501,10 +521,16 @@
     with jax.named_scope("drain"):
         for buf, part, sem in (
             (metas, peers, meta_send), (conv_out, pl.ds(0, n_tp - 1), conv_send),
-            (conv_out, (0, pl.ds(0, 2 * HALO)), halo_send), (staged, blocks, disp_send),
+            (staged, blocks, disp_send),
             (results, pl.ds(0, n_sp * (n_tp - 1) * cap), ret_send),
         ):
             remote(buf.at[part], buf.at[part], sem, halo_recv.at[0], right).wait_send()
+
+        @pl.when(has_next)
+        def _():
+            both = conv_out.at[0, pl.ds(0, 2 * HALO)]
+            remote(both, both, halo_send, halo_recv.at[0], right).wait_send()
+
     with jax.named_scope("red_wait_last"):
         for way in range(2):
             for h in range(2):

time: 106 us -> 105 us (level)
  no operation moved by 1% of the time
where the time goes in v4:
time: 105 us
  Pallas kernels  104 us (99%)
    pallas_call x1, Pallas kernels, body(): pl.pallas_call(functools.partial(experts_kernel, n_sp, n_tp, cap, top), o...  104 us

profile of v4, /device:TPU:0, one launch (start us, length us, event | category | flops | bytes accessed | tf_op | source)
XLA Modules:
  0.0 104.8 jit_solution(12467055075173586106)
XLA Ops:
  0.0 104.0 %shard_map.154 = bf16[128,2048]{1,0:T(8,128)(2,1)S(1)} custom-call(bf16[512,384]{1,0:T(8,128)(2,1)} %og_hbm.1, bf16[512,384]{1,0:T(8,128)(2,1)} %ig_hbm.1, bf16[512,384]{1,0:T(8,128)(2,1)} %cv_hbm.1, f32[3,384]{1,0:T(4,128)} %taps_hbm.1, f32[1536]{0:T(1024)} %mix_gain_hbm.1, bf16[128,2048]{1,0:T(8,128)(2,1)} %residual_hbm.1, f32[1,2048]{1,0:T(1,128)} %bitcast.3, ...), custom_call_target="tpu_custom_call" | custom-call | tf_op jit(solution)/shard_map/pallas_call | solution.py:575
  104.0 0.8 copy.18

commit v5 on v4

--- a/solution.py
+++ b/solution.py
@@ -507,7 +507,7 @@
             give_back(2 * s - 1, 0)
             give_back(2 * s, 1)
 
-        @pl.when(s == 1)
+        @pl.when(s == 0)
         def _():
             give_back(0, 0)
             give_back(0, 1)

time: 105 us -> 105 us (level)
  no operation moved by 1% of the time
where the time goes in v5:
time: 105 us
  Pallas kernels  104 us (99%)
    pallas_call x1, Pallas kernels, body(): pl.pallas_call(functools.partial(experts_kernel, n_sp, n_tp, cap, top), o...  104 us

profile of v5, /device:TPU:0, one launch (start us, length us, event | category | flops | bytes accessed | tf_op | source)
XLA Modules:
  0.0 104.8 jit_solution(11841368027365153183)
XLA Ops:
  0.0 104.0 %shard_map.154 = bf16[128,2048]{1,0:T(8,128)(2,1)S(1)} custom-call(bf16[512,384]{1,0:T(8,128)(2,1)} %og_hbm.1, bf16[512,384]{1,0:T(8,128)(2,1)} %ig_hbm.1, bf16[512,384]{1,0:T(8,128)(2,1)} %cv_hbm.1, f32[3,384]{1,0:T(4,128)} %taps_hbm.1, f32[1536]{0:T(1024)} %mix_gain_hbm.1, bf16[128,2048]{1,0:T(8,128)(2,1)} %residual_hbm.1, f32[1,2048]{1,0:T(1,128)} %bitcast.3, ...), custom_call_target="tpu_custom_call" | custom-call | tf_op jit(solution)/shard_map/pallas_call | solution.py:575
  104.0 0.8 copy.18
